TPU v7x, 32 devices: a whole 2x2x4 slice. The times are simulated.
32 devices in a mesh: grp: 2 (over y), fs: 4 (over z), tp: 4 (over x, core).
Axes of the slice: x: 2, y: 2, z: 4, core: 2. Of those that a mesh axis runs over, the one named last changes fastest.
Arguments:
- tokens: bfloat16 [4096, 2048], P(('grp', 'fs', 'tp')), parts along dimension 0, may hold values from -6 to 6
- route_ids: int32 [4096, 8], P(('grp', 'fs', 'tp')), parts along dimension 0, may hold values from 0 to 15, all different within a row; in each aligned block of 128 rows (0 to 127, 128 to 255, ...) at most 96 rows name the same one
- route_scores: float32 [4096, 8], P(('grp', 'fs', 'tp')), parts along dimension 0, may hold values from 0.05 to 1
- norm_gain: float32 [2048], P('fs'), may hold values from 0.1 to 1.9
- expert_gate: float32 [16, 2048, 256], P(None, 'fs', 'tp'), may hold values from -0.125 to 0.125
- expert_up: float32 [16, 2048, 256], P(None, 'fs', 'tp'), may hold values from -0.125 to 0.125
- expert_down: float32 [16, 256, 2048], P(None, 'fs', 'tp'), may hold values from -0.375 to 0.375
- shared_gate: float32 [2048, 256], P('fs', 'tp'), may hold values from -0.125 to 0.125
- shared_up: float32 [2048, 256], P('fs', 'tp'), may hold values from -0.125 to 0.125
- shared_down: float32 [256, 2048], P('fs', 'tp'), may hold values from -0.375 to 0.375
Outputs:
- mixed: bfloat16 [4096, 2048], P(('grp', 'fs', 'tp')), parts along dimension 0
- sampler_gate: bfloat16 [32, 2048, 256], P(('grp', 'fs', 'tp')), parts along dimension 0
- sampler_up: bfloat16 [32, 2048, 256], P(('grp', 'fs', 'tp')), parts along dimension 0
- sampler_down: bfloat16 [32, 256, 2048], P(('grp', 'fs', 'tp')), parts along dimension 0
- sampler_shared_gate: bfloat16 [4096, 256], P(('grp', 'fs')), parts along dimension 0
- sampler_shared_up: bfloat16 [4096, 256], P(('grp', 'fs')), parts along dimension 0
- sampler_shared_down: bfloat16 [512, 2048], P(('grp', 'fs')), parts along dimension 0
There are 2 independent parts, one for each index of `grp`. A program takes and returns all parts, laid end to end along the dimension named above; an argument that names none is the same for every part. Nothing has to cross between parts.
Inputs may be any that keep to these rules, and one draw needn't show every extreme that they name: `route_ids`: each row names 8 different experts. Among the 128 rows of one device no expert is named more than 96 times, a bound that some block reaches.
All inputs are finite; a program needn't handle non-finite values.
Results may differ from a plain program's by a relative error of at most 0.0084.
Values may be sent and summed in bfloat16 or wider, within the bound.
A program may use at most 128 MiB of HBM per device.

v0:
```python
import jax
import jax.numpy as jnp
from jax import lax
from jax.sharding import PartitionSpec as P

EPSILON = 1e-06
route_scale = 2.5


def expert_rows(row_block, w_gate, w_up, w_down):
    gate_rows = jnp.dot(row_block, w_gate, preferred_element_type=jnp.float32)
    up_rows = jnp.dot(row_block, w_up, preferred_element_type=jnp.float32)
    hidden = (jax.nn.silu(gate_rows) * up_rows).astype(jnp.bfloat16)
    return jnp.dot(hidden, w_down, preferred_element_type=jnp.float32).astype(jnp.bfloat16)


def relayout(arrived, fs_count, tp_count):
    tile_rows = arrived.shape[2]
    tile_cols = arrived.shape[3]
    grid = arrived.reshape(fs_count, tp_count, tile_rows, tile_cols)
    grid = jnp.transpose(grid, (0, 2, 1, 3))
    return grid.reshape(1, fs_count * tile_rows, tp_count * tile_cols)


def dispatch_plan(
    tokens,
    route_ids,
    route_scores,
    norm_gain,
    expert_gate,
    expert_up,
    expert_down,
    shared_gate,
    shared_up,
    shared_down,
):
    fs_count = lax.axis_size("fs")
    tp_count = lax.axis_size("tp")
    experts = fs_count * tp_count
    gain_col = norm_gain[:, None]
    piece_gate = (gain_col[None] * expert_gate).astype(jnp.bfloat16)
    piece_up = (gain_col[None] * expert_up).astype(jnp.bfloat16)
    piece_down = expert_down.astype(jnp.bfloat16)
    moved = (
        lax.all_to_all(piece_gate[:, None], ("fs", "tp"), split_axis=0, concat_axis=1, tiled=True),
        lax.all_to_all(piece_up[:, None], ("fs", "tp"), split_axis=0, concat_axis=1, tiled=True),
        lax.all_to_all(piece_down[:, None], ("fs", "tp"), split_axis=0, concat_axis=1, tiled=True),
    )
    served_gate = relayout(moved[0], fs_count, tp_count)
    served_up = relayout(moved[1], fs_count, tp_count)
    served_down = relayout(moved[2], fs_count, tp_count)
    tile_gate = (gain_col * shared_gate).astype(jnp.bfloat16)
    tile_up = (gain_col * shared_up).astype(jnp.bfloat16)
    tile_down = shared_down.astype(jnp.bfloat16)
    held_gate, held_up, held_down = (
        lax.all_gather(tile_gate, "tp", axis=1, tiled=True),
        lax.all_gather(tile_up, "tp", axis=1, tiled=True),
        lax.all_gather(tile_down, "tp", axis=1, tiled=True),
    )
    rows_dev = tokens.shape[0]
    width = tokens.shape[1]
    picks = route_ids.shape[1]
    capacity = 3 * rows_dev * picks // (2 * experts)
    widened = tokens.astype(jnp.float32)
    normed = (
        widened * lax.rsqrt(jnp.mean(widened * widened, axis=1, keepdims=True) + EPSILON)
    ).astype(jnp.bfloat16)
    weights = route_scale * route_scores / jnp.sum(route_scores, axis=1, keepdims=True)
    flat_ids = route_ids.reshape(-1)
    onehot = (flat_ids[:, None] == jnp.arange(experts, dtype=jnp.int32)[None, :]).astype(jnp.int32)
    earlier = jnp.cumsum(onehot, axis=0) - onehot
    ranks = jnp.sum(earlier * onehot, axis=1)
    target = flat_ids * capacity + ranks
    outbox = (
        jnp.zeros((experts * capacity, width), jnp.bfloat16)
        .at[target]
        .set(jnp.repeat(normed, picks, axis=0))
    )
    arrived = lax.all_to_all(
        outbox.reshape(experts, capacity, width),
        ("fs", "tp"),
        split_axis=0,
        concat_axis=0,
        tiled=True,
    )
    finished = expert_rows(
        arrived.reshape(-1, width), served_gate[0], served_up[0], served_down[0]
    ).reshape(arrived.shape)
    returned = lax.all_to_all(finished, ("fs", "tp"), split_axis=0, concat_axis=0, tiled=True)
    results = returned.reshape(experts * capacity, width)[target]
    routed = jnp.sum(
        results.reshape(rows_dev, picks, width).astype(jnp.float32) * weights[:, :, None], axis=1
    )
    columns = normed
    gate_part = jnp.dot(
        columns,
        lax.all_gather(held_gate, "fs", axis=0, tiled=True),
        preferred_element_type=jnp.float32,
    )
    up_part = jnp.dot(
        columns,
        lax.all_gather(held_up, "fs", axis=0, tiled=True),
        preferred_element_type=jnp.float32,
    )
    shared_hidden = (jax.nn.silu(gate_part) * up_part).astype(jnp.bfloat16)
    columns = shared_hidden
    shared_term = jnp.dot(
        columns,
        lax.all_gather(held_down, "fs", axis=0, tiled=True),
        preferred_element_type=jnp.float32,
    )
    mixed = (routed + shared_term).astype(jnp.bfloat16)
    return (mixed, served_gate, served_up, served_down, held_gate, held_up, held_down)


def dense_plan(
    tokens,
    route_ids,
    route_scores,
    norm_gain,
    expert_gate,
    expert_up,
    expert_down,
    shared_gate,
    shared_up,
    shared_down,
):
    fs_count = lax.axis_size("fs")
    tp_count = lax.axis_size("tp")
    experts = fs_count * tp_count
    both = ("fs", "tp")
    rows_dev, width = tokens.shape
    widened = tokens.astype(jnp.float32)
    normed = (
        widened * lax.rsqrt(jnp.mean(widened * widened, axis=1, keepdims=True) + EPSILON)
    ).astype(jnp.bfloat16)
    weights = route_scale * route_scores / jnp.sum(route_scores, axis=1, keepdims=True)
    named = route_ids[:, :, None] == jnp.arange(experts, dtype=jnp.int32)[None, None, :]
    shares = jnp.sum(jnp.where(named, weights[:, :, None], 0.0), axis=1)
    gain_col = norm_gain[:, None]
    cols = expert_gate.shape[2]
    shared_cols = shared_gate.shape[1]
    lanes = 2 * shared_cols
    tile_pair = jnp.concatenate([gain_col * shared_gate, gain_col * shared_up], axis=1).astype(
        jnp.bfloat16
    )
    pair_rows = tile_pair.shape[0]
    down_rows, down_cols = shared_down.shape
    strips = down_cols // lanes
    tile_down = jnp.transpose(
        shared_down.astype(jnp.bfloat16).reshape(down_rows, strips, lanes), (1, 0, 2)
    ).reshape(strips * down_rows, lanes)
    tiles = lax.all_gather(jnp.concatenate([tile_pair, tile_down], axis=0), both, axis=0, tiled=False)
    tiles = tiles.reshape(fs_count, tp_count, pair_rows + strips * down_rows, lanes)
    whole_gate = jnp.transpose(tiles[:, :, :pair_rows, :shared_cols], (0, 2, 1, 3)).reshape(
        fs_count * pair_rows, tp_count * shared_cols
    )
    whole_up = jnp.transpose(tiles[:, :, :pair_rows, shared_cols:], (0, 2, 1, 3)).reshape(
        fs_count * pair_rows, tp_count * shared_cols
    )
    whole_down = jnp.transpose(
        tiles[:, :, pair_rows:].reshape(fs_count, tp_count, strips, down_rows, lanes),
        (0, 3, 1, 2, 4),
    ).reshape(fs_count * down_rows, tp_count * down_cols)
    place = lax.axis_index("fs")
    held_gate = lax.dynamic_slice_in_dim(whole_gate, place * pair_rows, pair_rows, 0)
    held_up = lax.dynamic_slice_in_dim(whole_up, place * pair_rows, pair_rows, 0)
    held_down = lax.dynamic_slice_in_dim(whole_down, place * down_rows, down_rows, 0)

    all_normed = lax.all_gather(
        lax.all_gather(normed, "fs", axis=0, tiled=True), "tp", axis=0, tiled=True
    )
    own_share = lax.all_to_all(
        shares.T.reshape(experts, 1, rows_dev), both, split_axis=0, concat_axis=1, tiled=True
    ).reshape(fs_count, tp_count, rows_dev)
    own_share = jnp.transpose(own_share, (1, 0, 2)).reshape(-1)

    piece_gate = (gain_col[None] * expert_gate).astype(jnp.bfloat16)
    piece_up = (gain_col[None] * expert_up).astype(jnp.bfloat16)
    piece_pair = jnp.concatenate([piece_gate, piece_up], axis=2)
    piece_down = expert_down.astype(jnp.bfloat16)
    pair = lax.all_to_all(piece_pair[:, None], both, split_axis=0, concat_axis=1, tiled=True)
    down = lax.all_to_all(piece_down[:, None], both, split_axis=0, concat_axis=1, tiled=True)
    served_gate = relayout(pair[:, :, :, :cols], fs_count, tp_count)
    served_up = relayout(pair[:, :, :, cols:], fs_count, tp_count)
    served_down = relayout(down, fs_count, tp_count)
    gate_rows = jnp.dot(all_normed, served_gate[0], preferred_element_type=jnp.float32)
    up_rows = jnp.dot(all_normed, served_up[0], preferred_element_type=jnp.float32)
    hidden = (jax.nn.silu(gate_rows) * up_rows).astype(jnp.bfloat16)
    produced = jnp.dot(hidden, served_down[0], preferred_element_type=jnp.float32)
    partial = (produced * own_share[:, None]).astype(jnp.bfloat16)
    routed = lax.psum_scatter(partial, "tp", scatter_dimension=0, tiled=True)
    routed = lax.psum_scatter(routed, "fs", scatter_dimension=0, tiled=True)

    gate_part = jnp.dot(normed, whole_gate, preferred_element_type=jnp.float32)
    up_part = jnp.dot(normed, whole_up, preferred_element_type=jnp.float32)
    shared_hidden = (jax.nn.silu(gate_part) * up_part).astype(jnp.bfloat16)
    shared_term = jnp.dot(shared_hidden, whole_down, preferred_element_type=jnp.float32)
    mixed = (routed.astype(jnp.float32) + shared_term).astype(jnp.bfloat16)
    return (mixed, served_gate, served_up, served_down, held_gate, held_up, held_down)


def on_device(*args):
    experts = lax.axis_size("fs") * lax.axis_size("tp")
    picks = args[1].shape[1]
    if experts <= 4 * picks:
        return dense_plan(*args)
    return dispatch_plan(*args)


def solution(mesh):
    return jax.shard_map(
        on_device,
        mesh=mesh,
        in_specs=(
            P(("grp", "fs", "tp"), None),
            P(("grp", "fs", "tp"), None),
            P(("grp", "fs", "tp"), None),
            P("fs"),
            P(None, "fs", "tp"),
            P(None, "fs", "tp"),
            P(None, "fs", "tp"),
            P("fs", "tp"),
            P("fs", "tp"),
            P("fs", "tp"),
        ),
        out_specs=(
            P(("grp", "fs", "tp"), None),
            P(("grp", "fs", "tp"), None, None),
            P(("grp", "fs", "tp"), None, None),
            P(("grp", "fs", "tp"), None, None),
            P(("grp", "fs"), None),
            P(("grp", "fs"), None),
            P(("grp", "fs"), None),
        ),
        check_vma=False,
    )
```

profile of v0, /device:TPU:0, one launch (start us, length us, event | category | flops | bytes accessed | tf_op | source)
XLA Modules:
  0.0 313.2 jit_solution(11789254881723399388)
XLA Ops:
  8.1 1.4 fusion.3
  9.5 2.0 fusion.4
  11.5 48.5 %all-gather.5.cloned.1.call-done = bf16[512,2048]{1,0:T(8,128)(2,1)} async-done(((bf16[128,2048]{1,0:T(8,128)(2,1)}), bf16[512,2048]{1,0:T(8,128)(2,1)}) %all-gather.5.cloned.1.call-update) | async-done | bytes 2097168 | tf_op jit(solution)/shard_map/all_gather | solution.py:171
  60.7 3.5 %all-to-all-start.2 = ((f32[16,1,128]{2,1,0:T(1,128)}), f32[16,1,128]{2,1,0:T(1,128)S(1)}, u32[]{:S(2)}, u32[]{:S(2)}) async-start(f32[16,1,128]{2,1,0:T(1,128)} %bitcast.11), calls=%async_computation.2 | async-start | bytes 16384 | tf_op jit(solution)/shard_map/all_to_all | solution.py:173
  65.4 5.2 %all-to-all-done.2 = f32[16,1,128]{2,1,0:T(1,128)S(1)} async-done(((f32[16,1,128]{2,1,0:T(1,128)}), f32[16,1,128]{2,1,0:T(1,128)S(1)}, u32[]{:S(2)}, u32[]{:S(2)}) %all-to-all-start.2) | async-done | bytes 8224 | tf_op jit(solution)/shard_map/all_to_all | solution.py:173
  70.6 3.7 %all-to-all-start.1 = ((bf16[16,1,64,512]{3,2,1,0:T(8,128)(2,1)}), bf16[16,1,64,512]{3,2,1,0:T(8,128)(2,1)S(1)}, u32[]{:S(2)}, u32[]{:S(2)}) async-start(bf16[16,1,64,512]{3,2,1,0:T(8,128)(2,1)} %convert_bitcast_fusion), calls=%async_computation.1 | async-start | bytes 2097152 | tf_op jit(solution)/shard_map/all_to_all | solution.py:183
  74.3 2.2 multiply_convert_fusion.2
  76.5 1.5 maximum_bitcast_fusion
  77.9 19.2 %all-to-all-done.1 = bf16[16,1,64,512]{3,2,1,0:T(8,128)(2,1)S(1)} async-done(((bf16[16,1,64,512]{3,2,1,0:T(8,128)(2,1)}), bf16[16,1,64,512]{3,2,1,0:T(8,128)(2,1)S(1)}, u32[]{:S(2)}, u32[]{:S(2)}) %all-to-all-start.1) | async-done | bytes 1048608 | tf_op jit(solution)/shard_map/all_to_all | solution.py:183
  97.1 6.8 %all-to-all-start = ((bf16[16,1,512,128]{2,3,1,0:T(8,128)(2,1)}), bf16[16,1,512,128]{2,3,1,0:T(8,128)(2,1)S(1)}, u32[]{:S(2)}, u32[]{:S(2)}) async-start(bf16[16,1,512,128]{2,3,1,0:T(8,128)(2,1)} %maximum_bitcast_fusion), calls=%async_computation | async-start | bytes 4194304 | tf_op jit(solution)/shard_map/all_to_all | solution.py:182
  104.0 2.0 copy.113
  106.1 1.2 copy.104
  107.3 37.7 %all-to-all-done = bf16[16,1,512,128]{2,3,1,0:T(8,128)(2,1)S(1)} async-done(((bf16[16,1,512,128]{2,3,1,0:T(8,128)(2,1)}), bf16[16,1,512,128]{2,3,1,0:T(8,128)(2,1)S(1)}, u32[]{:S(2)}, u32[]{:S(2)}) %all-to-all-start) | async-done | bytes 2097184 | tf_op jit(solution)/shard_map/all_to_all | solution.py:182
  146.1 1.2 copy.102
  148.2 1.2 copy.103
  149.4 3.0 all-gather.7.cloned.1.call-done
  152.4 7.3 %fusion.15 = f32[2048,256]{1,0:T(8,128)} fusion(bf16[2048,2048]{1,0:T(8,128)(2,1)} %all-gather.7.cloned.1.call-done, bf16[2048,256]{0,1:T(8,128)(2,1)} %bitcast.94), kind=kOutput, calls=%fused_computation.40 | convolution fusion | flops 2147483648 | bytes 11534336 | tf_op jit(solution)/shard_map/dot_general | solution.py:187
  159.7 13.8 %multiply_convert_fusion = bf16[2048,2048]{1,0:T(8,128)(2,1)} fusion(bf16[256,2048]{1,0:T(8,128)(2,1)} %bitcast.92, f32[2048]{0:T(1024)S(1)} %bitcast.98, bf16[2048,2048]{1,0:T(8,128)(2,1)} %all-gather.7.cloned.1.call-done, bf16[2048,256]{0,1:T(8,128)(2,1)} %bitcast.93, f32[2048,256]{1,0:T(8,128)} %fusion.15), kind=kOutput, calls=%fused_computation | convolution fusion | flops 4306501632 | bytes 20979712 | tf_op jit(solution)/shard_map/dot_general | solution.py:190
  175.7 81.5 %reduce-scatter.3.cloned.1.call-done = bf16[512,2048]{1,0:T(8,128)(2,1)} async-done(((bf16[2048,2048]{1,0:T(8,128)(2,1)}), bf16[512,2048]{1,0:T(8,128)(2,1)}) %reduce-scatter.3.cloned.1.call-update) | async-done | bytes 2097168 | tf_op jit(solution)/shard_map/reduce_scatter | solution.py:192
  257.2 1.6 reshape.98
  259.6 1.3 copy.98
  261.7 1.3 copy.99
  263.0 3.6 %copy.94 = bf16[12288,128]{1,0:T(8,128)(2,1)S(1)} copy(bf16[12288,128]{0,1:T(8,128)(2,1)} %all-gather.9.cloned.1.call-done) | data formatting | bytes 6291456 | tf_op jit(solution)/shard_map/all_gather | solution.py:153
  267.7 2.8 slice_bitcast_fusion.1
  270.5 4.2 %copy.95 = bf16[4,512,4,64]{1,0,3,2:T(4,128)(2,1)} copy(bf16[4,512,4,64]{3,1,2,0:T(8,128)(2,1)} %get-tuple-element.42) | data formatting | bytes 2097152 | tf_op jit(solution)/shard_map/transpose | solution.py:155
  274.7 1.5 copy.105
  276.2 2.3 copy.96
  278.6 2.6 copy.106
  281.2 1.8 copy.97
  282.9 1.9 reshape.95
  288.7 14.2 %reduce-scatter.5.cloned.1.call-done = bf16[128,2048]{1,0:T(8,128)(2,1)} async-done(((bf16[512,2048]{1,0:T(8,128)(2,1)}), bf16[128,2048]{1,0:T(8,128)(2,1)}) %reduce-scatter.5.cloned.1.call-update) | async-done | bytes 524304 | tf_op jit(solution)/shard_map/reduce_scatter | solution.py:193
  303.0 3.1 fusion.1
  (56 shorter events, 12.4 us)
Async XLA Ops:
  8.0 52.0 %copy-start.8 = (f32[128,8]{0,1:T(8,128)S(1)}, f32[128,8]{0,1:T(8,128)}, u32[]{:S(2)}) copy-start(f32[128,8]{0,1:T(8,128)} %param.12) | copy-start | bytes 12292
  8.0 52.1 %copy-start.10 = (s32[128,8]{0,1:T(8,128)S(1)}, s32[128,8]{0,1:T(8,128)}, u32[]{:S(2)}) copy-start(s32[128,8]{0,1:T(8,128)} %param.11) | copy-start | bytes 12292
  8.0 56.2 %copy-start.4 = (f32[16,64,512]{2,1,0:T(8,128)S(1)}, f32[16,64,512]{2,1,0:T(8,128)}, u32[]{:S(2)}) copy-start(f32[16,64,512]{2,1,0:T(8,128)} %param.16) | copy-start | bytes 6291460
  8.0 52.0 %all-gather.5.cloned.1.call-start = ((), (), s32[]{:S(2)}) async-start(), calls=%async_computation.5 | async-start | bytes 2621440 | tf_op jit(solution)/shard_map/all_gather | solution.py:171
  11.5 140.9 %all-gather.7.cloned.1.call-start = ((), (), s32[]{:S(2)}) async-start(), calls=%async_computation.6 | async-start | bytes 10485760 | tf_op jit(solution)/shard_map/all_gather | solution.py:170
  60.7 9.9 %all-to-all-start.2 = ((f32[16,1,128]{2,1,0:T(1,128)}), f32[16,1,128]{2,1,0:T(1,128)S(1)}, u32[]{:S(2)}, u32[]{:S(2)}) async-start(f32[16,1,128]{2,1,0:T(1,128)} %bitcast.11), calls=%async_computation.2 | async-start | bytes 16384 | tf_op jit(solution)/shard_map/all_to_all | solution.py:173
  64.2 10.0 %copy-start.9 = (f32[512]{0:T(512)S(1)}, f32[512]{0:T(512)}, u32[]{:S(2)}) copy-start(f32[512]{0:T(512)} %param.13) | copy-start | bytes 6148
  65.4 8.9 %copy-start.5 = (f32[16,512,64]{1,2,0:T(8,128)S(1)}, f32[16,512,64]{1,2,0:T(8,128)}, u32[]{:S(2)}) copy-start(f32[16,512,64]{1,2,0:T(8,128)} %param.14) | copy-start | bytes 6291460
  70.6 26.5 %all-to-all-start.1 = ((bf16[16,1,64,512]{3,2,1,0:T(8,128)(2,1)}), bf16[16,1,64,512]{3,2,1,0:T(8,128)(2,1)S(1)}, u32[]{:S(2)}, u32[]{:S(2)}) async-start(bf16[16,1,64,512]{3,2,1,0:T(8,128)(2,1)} %convert_bitcast_fusion), calls=%async_computation.1 | async-start | bytes 2097152 | tf_op jit(solution)/shard_map/all_to_all | solution.py:183
  97.1 6.9 %copy-start.2 = (bf16[16,1,64,512]{3,2,1,0:T(8,128)(2,1)}, bf16[16,1,64,512]{3,2,1,0:T(8,128)(2,1)S(1)}, u32[]{:S(2)}) copy-start(bf16[16,1,64,512]{3,2,1,0:T(8,128)(2,1)S(1)} %all-to-all-done.1) | copy-start | bytes 3145732
  97.1 47.9 %all-to-all-start = ((bf16[16,1,512,128]{2,3,1,0:T(8,128)(2,1)}), bf16[16,1,512,128]{2,3,1,0:T(8,128)(2,1)S(1)}, u32[]{:S(2)}, u32[]{:S(2)}) async-start(bf16[16,1,512,128]{2,3,1,0:T(8,128)(2,1)} %maximum_bitcast_fusion), calls=%async_computation | async-start | bytes 4194304 | tf_op jit(solution)/shard_map/all_to_all | solution.py:182
  104.0 153.2 %reduce-scatter.3.cloned.1.call-start = ((), (), s32[]{:S(2)}) async-start(), calls=%async_computation.7 | async-start | bytes 10485760 | tf_op jit(solution)/shard_map/reduce_scatter | solution.py:192
  173.5 1.3 copy-start.6
  173.5 1.3 copy-start.7
  173.6 89.4 %all-gather.9.cloned.1.call-start = ((), (), s32[]{:S(2)}) async-start(), calls=%async_computation.9 | async-start | bytes 3342336 | tf_op jit(solution)/shard_map/all_gather | solution.py:153
  175.6 127.3 %reduce-scatter.5.cloned.1.call-start = ((), (), s32[]{:S(2)}) async-start(), calls=%async_computation.8 | async-start | bytes 2621440 | tf_op jit(solution)/shard_map/reduce_scatter | solution.py:193
  270.5 5.7 %copy-start = (bf16[4,512,4,64]{3,1,2,0:T(8,128)(2,1)S(1)}, bf16[4,512,4,64]{3,1,2,0:T(8,128)(2,1)}, u32[]{:S(2)}) copy-start(bf16[4,512,4,64]{3,1,2,0:T(8,128)(2,1)} %get-tuple-element.43) | copy-start | bytes 3145732
  278.6 2.6 copy-start.3
  282.9 5.3 %copy-start.1 = (bf16[128,2048]{1,0:T(8,128)(2,1)S(1)}, bf16[128,2048]{1,0:T(8,128)(2,1)}, u32[]{:S(2)}) copy-start(bf16[128,2048]{1,0:T(8,128)(2,1)} %fusion.4) | copy-start | bytes 1572868
Sparse Core Ops, SparseCore 0:
  11.6 48.3 all-gather.4
  61.6 90.7 all-gather.6
  173.7 83.4 reduce-scatter.2
  259.3 43.6 reduce-scatter.4
Sparse Core Ops, SparseCore 1:
  176.8 65.5 all-gather.8
where the time goes:
time: 314 us; the launch traced here: 313 us
  waiting for transfers between devices  209 us (67%)
  local copies, waits for them, and re-layouts  38.8 us (12%)
  matrix products  24.7 us (8%)
  between operations  15.5 us (5%)
  starting transfers between devices  14.4 us (5%)
  other arithmetic  10.4 us (3%)
    reduce_scatter x1, waiting for transfers between devices, dense_plan(): routed = lax.psum_scatter(partial, 'tp', scatter_dimension=0, tiled=True)  81.5 us
    all_gather x1, waiting for transfers between devices, dense_plan(): lax.all_gather(normed, 'fs', axis=0, tiled=True)  48.5 us
    all_to_all x1, waiting for transfers between devices, dense_plan(): lax.all_to_all(piece_pair[:, None], both, split_axis=0, concat_axis=1, ti...  37.7 us
    all_to_all x1, waiting for transfers between devices, dense_plan(): lax.all_to_all(piece_down[:, None], both, split_axis=0, concat_axis=1, ti...  19.2 us
    reduce_scatter x1, waiting for transfers between devices, dense_plan(): routed = lax.psum_scatter(routed, 'fs', scatter_dimension=0, tiled=True)  14.2 us
    dot_general x1, matrix products, dense_plan(): jnp.dot(hidden, served_down[0], preferred_element_type=jnp.float32)  13.8 us
    unnamed x31, local copies, waits for them, and re-layouts  12.2 us
    dot_general x1, matrix products, dense_plan(): jnp.dot(all_normed, served_gate[0], preferred_element_type=jnp.float32)  7.33 us
  transfers between devices with their start and end apart: 8, of which 7 were waited for; matrix products, arithmetic and copies ran while one was open for 15% of the time, Pallas kernels for 0%

commit v1 on v0

--- a/solution.py
+++ b/solution.py
@@ -1,10 +1,15 @@
+import functools
 import jax
 import jax.numpy as jnp
 from jax import lax
+from jax.experimental import pallas as pl
+from jax.experimental.pallas import tpu as pltpu
 from jax.sharding import PartitionSpec as P
 
 EPSILON = 1e-06
 route_scale = 2.5
+CORES = 2
+MESH = pl.DeviceIdType.MESH
 
 
 def expert_rows(row_block, w_gate, w_up, w_down):
@@ -113,7 +118,518 @@
     return (mixed, served_gate, served_up, served_down, held_gate, held_up, held_down)
 
 
-def dense_plan(
+def handover_kernel(
+    nz,
+    nt,
+    normed,
+    gu,
+    dn,
+    sgu,
+    sdn,
+    shares,
+    o_mix,
+    o_w,
+    o_hgu,
+    o_hd,
+    w,
+    tok,
+    part,
+    rd,
+    rx,
+    rz,
+    share,
+    hgu,
+    hd,
+    mix,
+    lsem,
+    wsend,
+    wrecv,
+    ysend,
+    yrecv,
+    shsend,
+    shrecv,
+    ssend,
+    srecv,
+    hsend,
+    hrecv,
+    asend,
+    arecv,
+    rdsend,
+    rdrecv,
+    rxsend,
+    rxrecv,
+    rzsend,
+    rzrecv,
+):
+    n = nz * nt
+    xc = nt // CORES
+    g = lax.axis_index("grp")
+    z = lax.axis_index("fs")
+    t = lax.axis_index("tp")
+    x = t // CORES
+    c = t % CORES
+    me = z * nt + t
+    rows, width = normed.shape
+    ft, dt = gu.shape[2], gu.shape[3]
+    fr, dc = dn.shape[1], dn.shape[2]
+    inner = o_w.shape[1]
+    sd = w.shape[1] - inner
+    half_f, half_r = ft // 2, fr // 2
+
+    def dev(zz, tt, gg=None):
+        return {"grp": g if gg is None else gg, "fs": zz, "tp": tt}
+
+    def rem(src, dst, ssem, rsem, device):
+        return pltpu.make_async_remote_copy(
+            src_ref=src,
+            dst_ref=dst,
+            send_sem=ssem,
+            recv_sem=rsem,
+            device_id=device,
+            device_id_type=MESH,
+        )
+
+    def al(v, m):
+        return pl.multiple_of(v, m)
+
+    partner = dev(z, x * CORES + 1 - c)
+    across = dev(z, t, 1 - g)
+
+    def xdev(k):
+        return dev(z, lax.rem(x + k, xc) * CORES + c)
+
+    def slot(p, h, xb):
+        return p * nt + h * xc + xb
+
+    barrier = pltpu.get_barrier_semaphore()
+
+    @pl.loop(1, n)
+    def _(k):
+        j = lax.rem(me + k, n)
+        pl.semaphore_signal(barrier, 1, device_id=dev(j // nt, j % nt), device_id_type=MESH)
+
+    pl.semaphore_signal(barrier, 1, device_id=across, device_id_type=MESH)
+    pl.semaphore_wait(barrier, n)
+
+    def gu_at(src):
+        zs, ts = src // nt, src % nt
+        return lambda gg: w.at[
+            pl.ds(0, 2), pl.ds(al(ts * ft + gg * half_f, half_f), half_f), pl.ds(al(zs * dt, dt), dt)
+        ]
+
+    def dn_at(src):
+        zs, ts = src // nt, src % nt
+        return lambda gg: w.at[
+            2, pl.ds(al(zs * fr + gg * half_r, half_r), half_r), pl.ds(al(ts * dc, dc), dc)
+        ]
+
+    def w_send(j):
+        device = dev(j // nt, j % nt)
+        return (
+            rem(
+                gu.at[j, pl.ds(0, 2), pl.ds(al(g * half_f, half_f), half_f), :],
+                gu_at(me)(g),
+                wsend.at[0, j],
+                wrecv.at[0, me],
+                device,
+            ),
+            rem(
+                dn.at[j, pl.ds(al(g * half_r, half_r), half_r), :],
+                dn_at(me)(g),
+                wsend.at[1, j],
+                wrecv.at[1, me],
+                device,
+            ),
+        )
+
+    def w_across(s, gg):
+        return (
+            rem(gu_at(s)(gg), gu_at(s)(gg), ysend.at[0, s], yrecv.at[0, s], across),
+            rem(dn_at(s)(gg), dn_at(s)(gg), ysend.at[1, s], yrecv.at[1, s], across),
+        )
+
+    def share_send(j):
+        return rem(
+            shares.at[j], share.at[me], shsend.at[j], shrecv.at[me], dev(j // nt, j % nt)
+        )
+
+    def sgu_at(zs):
+        return w.at[pl.ds(0, 2), pl.ds(inner, sd), pl.ds(al(zs * dt, dt), dt)]
+
+    def sdn_at(ts):
+        return w.at[2, pl.ds(inner, sd), pl.ds(al(ts * dc, dc), dc)]
+
+    def sgu_send(k):
+        j = t * nz + k
+        return j, rem(
+            sgu.at[pl.ds(0, 2), pl.ds(k * sd, sd), :],
+            sgu_at(z),
+            ssend.at[0, k],
+            srecv.at[0, z],
+            dev(j // nt, j % nt),
+        )
+
+    def sdn_send(k):
+        j = z * nt + k
+        return j, rem(
+            sdn.at[pl.ds(k * sd, sd), :],
+            sdn_at(t),
+            ssend.at[1, k],
+            srecv.at[1, t],
+            dev(j // nt, j % nt),
+        )
+
+    def hgu_at(ts):
+        return hgu.at[pl.ds(0, 2), pl.ds(al(ts * ft, ft), ft), :]
+
+    def hd_at(ts):
+        return hd.at[:, pl.ds(al(ts * dc, dc), dc)]
+
+    def held_x(k):
+        return (
+            rem(sgu, hgu_at(t), hsend.at[0, k], hrecv.at[0, t], xdev(k)),
+            rem(sdn, hd_at(t), hsend.at[1, k], hrecv.at[1, t], xdev(k)),
+        )
+
+    def held_core(xb):
+        ts = xb * CORES + c
+        return (
+            rem(hgu_at(ts), hgu_at(ts), hsend.at[2, xb], hrecv.at[0, ts], partner),
+            rem(hd_at(ts), hd_at(ts), hsend.at[3, xb], hrecv.at[1, ts], partner),
+        )
+
+    def a_z(p, up):
+        s = slot(p, c, x)
+        return rem(
+            tok.at[s],
+            tok.at[s],
+            asend.at[0 if up else 1, s],
+            arecv.at[s],
+            dev(z + 1 if up else z - 1, t),
+        )
+
+    def a_x(p, k):
+        s = slot(p, c, x)
+        return rem(tok.at[s], tok.at[s], asend.at[2 + k, s], arecv.at[s], xdev(k))
+
+    def a_core(p, xb):
+        s = slot(p, c, xb)
+        return rem(tok.at[s], tok.at[s], asend.at[2, s], arecv.at[s], partner)
+
+    def a_wait(s):
+        rem(tok.at[s], tok.at[s], asend.at[2, s], arecv.at[s], partner).wait_recv()
+
+    def r_core(p):
+        return rem(
+            part.at[pl.ds(slot(p, 1 - c, 0), xc)],
+            rd.at[pl.ds(p * xc, xc)],
+            rdsend.at[p],
+            rdrecv.at[p],
+            partner,
+        )
+
+    def r_x(p, k):
+        xb = lax.rem(x + k, xc)
+        return rem(
+            part.at[slot(p, c, xb)],
+            rx.at[p * (xc - 1) + k - 1],
+            rxsend.at[p, k - 1],
+            rxrecv.at[p, k - 1],
+            xdev(k),
+        )
+
+    def r_z(p):
+        return rem(
+            part.at[slot(p, c, x)], rz.at[z], rzsend.at[p], rzrecv.at[z], dev(p, t)
+        )
+
+    own = slot(z, c, x)
+    locals_ = [
+        pltpu.make_async_copy(normed, tok.at[own], lsem.at[0]),
+        pltpu.make_async_copy(
+            gu.at[me],
+            w.at[pl.ds(0, 2), pl.ds(al(t * ft, ft), ft), pl.ds(al(z * dt, dt), dt)],
+            lsem.at[1],
+        ),
+        pltpu.make_async_copy(
+            dn.at[me],
+            w.at[2, pl.ds(al(z * fr, fr), fr), pl.ds(al(t * dc, dc), dc)],
+            lsem.at[2],
+        ),
+        pltpu.make_async_copy(sgu, hgu_at(t), lsem.at[3]),
+        pltpu.make_async_copy(sdn, hd_at(t), lsem.at[4]),
+        pltpu.make_async_copy(shares.at[me], share.at[me], lsem.at[5]),
+    ]
+    for cp in locals_:
+        cp.start()
+    self_gu = pltpu.make_async_copy(
+        sgu.at[pl.ds(0, 2), pl.ds(al((me % nz) * sd, sd), sd), :], sgu_at(z), lsem.at[6]
+    )
+    self_dn = pltpu.make_async_copy(
+        sdn.at[pl.ds(al((me % nt) * sd, sd), sd), :], sdn_at(t), lsem.at[7]
+    )
+
+    @pl.when(me // nz == t)
+    def _():
+        self_gu.start()
+
+    @pl.when(me // nt == z)
+    def _():
+        self_dn.start()
+
+    @pl.loop(1, n)
+    def _(k):
+        j = lax.rem(me + k, n)
+        for cp in w_send(j):
+            cp.start()
+        share_send(j).start()
+
+    for send, count in ((sgu_send, nz), (sdn_send, nt)):
+        for k in range(count):
+            j, cp = send(k)
+
+            @pl.when(j != me)
+            def _():
+                cp.start()
+
+    for cp in locals_:
+        cp.wait()
+    a_core(z, x).start()
+
+    @pl.when(z < nz - 1)
+    def _():
+        a_z(z, True).start()
+
+    @pl.when(z > 0)
+    def _():
+        a_z(z, False).start()
+
+    for k in range(1, xc):
+        a_x(z, k).start()
+
+    @pl.loop(1, n)
+    def _(k):
+        s = lax.rem(me + n - k, n)
+        for i, at in ((0, gu_at), (1, dn_at)):
+            rem(at(s)(g), at(s)(g), ysend.at[i, s], wrecv.at[i, s], across).wait_recv()
+        for cp in w_across(s, g):
+            cp.start()
+
+    @pl.loop(1, n)
+    def _(k):
+        s = lax.rem(me + n - k, n)
+        for cp in w_across(s, 1 - g):
+            cp.wait_recv()
+        rem(shares.at[s], share.at[s], shsend.at[s], shrecv.at[s], across).wait_recv()
+
+    for k in range(nz):
+        @pl.when(k * nt + me // nz != me)
+        def _():
+            rem(sgu_at(k), sgu_at(k), ssend.at[0, k], srecv.at[0, k], across).wait_recv()
+
+    for k in range(nt):
+        @pl.when((me // nt) * nt + k != me)
+        def _():
+            rem(sdn_at(k), sdn_at(k), ssend.at[1, k], srecv.at[1, k], across).wait_recv()
+
+    @pl.when(me // nz == t)
+    def _():
+        self_gu.wait()
+
+    @pl.when(me // nt == z)
+    def _():
+        self_dn.wait()
+
+    outs = [pltpu.make_async_copy(w.at[:, pl.ds(0, inner), :], o_w, lsem.at[0])]
+    outs[0].start()
+
+    nt_dims = (((1,), (1,)), ((), ()))
+
+    def compute(p, h):
+        first = slot(p, h, 0)
+        xs = tok[pl.ds(first, xc)].reshape(xc * rows, width)
+        gate = lax.dot_general(xs, w[0], nt_dims, preferred_element_type=jnp.float32)
+        up = lax.dot_general(xs, w[1], nt_dims, preferred_element_type=jnp.float32)
+        hidden = gate / (1.0 + jnp.exp(-gate)) * up
+        scale = jnp.concatenate(
+            [
+                jnp.transpose(jnp.broadcast_to(share[p * nt + xb * CORES + h], (rows, rows)))
+                for xb in range(xc)
+            ],
+            axis=0,
+        )[:, :1]
+        col = lax.broadcasted_iota(jnp.int32, hidden.shape, 1)
+        hidden = jnp.where(col < inner, hidden * scale, hidden).astype(jnp.bfloat16)
+        step = min(512, width)
+        for lo in range(0, width, step):
+            res = jnp.dot(hidden, w[2, :, lo : lo + step], preferred_element_type=jnp.float32)
+            part[pl.ds(first, xc), :, lo : lo + step] = res.astype(jnp.bfloat16).reshape(
+                xc, rows, step
+            )
+
+    steps = 2 * nz - 1
+
+    def plane(i):
+        d = (i + 1) // 2
+        p = z + d * (1 - 2 * (i % 2))
+        return p, (p >= 0) & (p < nz) & (i < steps)
+
+    def forward(i):
+        p, ok = plane(i)
+
+        @pl.when(ok & (i > 0))
+        def _():
+            a_wait(slot(p, c, x))
+
+            @pl.when((p < z) & (z < nz - 1))
+            def _():
+                a_z(p, True).start()
+
+            @pl.when((p > z) & (z > 0))
+            def _():
+                a_z(p, False).start()
+
+            a_core(p, x).start()
+            for k in range(1, xc):
+                a_x(p, k).start()
+
+    def work(i):
+        p, ok = plane(i)
+
+        @pl.when(ok)
+        def _():
+            for k in range(1, xc):
+                xb = lax.rem(x + k, xc)
+                a_wait(slot(p, c, xb))
+                a_core(p, xb).start()
+            for xb in range(xc):
+                a_wait(slot(p, 1 - c, xb))
+
+            @pl.loop(0, 2)
+            def _(j):
+                compute(p, (1 - c) * (1 - j) + c * j)
+
+                @pl.when(j == 0)
+                def _():
+                    r_core(p).start()
+
+            r_core(p).wait_recv()
+            for xb in range(xc):
+                s = slot(p, c, xb)
+                part[s] = (
+                    part[s].astype(jnp.float32) + rd[p * xc + xb].astype(jnp.float32)
+                ).astype(jnp.bfloat16)
+            for k in range(1, xc):
+                r_x(p, k).start()
+
+    def settle(i):
+        p, ok = plane(i)
+
+        @pl.when(ok & (i >= 0))
+        def _():
+            s = slot(p, c, x)
+            acc = part[s].astype(jnp.float32)
+            for k in range(1, xc):
+                r_x(p, k).wait_recv()
+                acc = acc + rx[p * (xc - 1) + k - 1].astype(jnp.float32)
+            part[s] = acc.astype(jnp.bfloat16)
+
+            @pl.when(p != z)
+            def _():
+                r_z(p).start()
+
+    @pl.loop(0, steps + 1)
+    def _(i):
+        work(i)
+        forward(i + 1)
+
+        @pl.when(i > 0)
+        def _():
+            settle(i - 1)
+
+    for k in range(1, xc):
+        for cp in held_x(k):
+            cp.start()
+    for cp in held_core(x):
+        cp.start()
+    for k in range(1, xc):
+        xb = lax.rem(x + k, xc)
+        ts = xb * CORES + c
+        rem(hgu_at(ts), hgu_at(ts), hsend.at[0, k], hrecv.at[0, ts], partner).wait_recv()
+        rem(hd_at(ts), hd_at(ts), hsend.at[1, k], hrecv.at[1, ts], partner).wait_recv()
+        for cp in held_core(xb):
+            cp.start()
+    for xb in range(xc):
+        ts = xb * CORES + 1 - c
+        rem(hgu_at(ts), hgu_at(ts), hsend.at[2, xb], hrecv.at[0, ts], partner).wait_recv()
+        rem(hd_at(ts), hd_at(ts), hsend.at[3, xb], hrecv.at[1, ts], partner).wait_recv()
+    outs.append(pltpu.make_async_copy(hgu, o_hgu, lsem.at[1]))
+    outs.append(pltpu.make_async_copy(hd, o_hd, lsem.at[2]))
+    outs[1].start()
+    outs[2].start()
+
+    for zs in range(nz):
+        @pl.when(zs != z)
+        def _():
+            rem(rz.at[zs], rz.at[zs], rzsend.at[zs], rzrecv.at[zs], partner).wait_recv()
+
+    acc = part[own].astype(jnp.float32)
+    for k in range(1, nz):
+        acc = acc + rz[lax.rem(z + k, nz)].astype(jnp.float32)
+    mix[...] = acc.astype(jnp.bfloat16)
+    outs.append(pltpu.make_async_copy(mix, o_mix, lsem.at[3]))
+    outs[3].start()
+
+    @pl.loop(1, n)
+    def _(k):
+        j = lax.rem(me + k, n)
+        for cp in w_send(j):
+            cp.wait_send()
+        share_send(j).wait_send()
+        for cp in w_across(j, g):
+            cp.wait_send()
+
+    for send, count in ((sgu_send, nz), (sdn_send, nt)):
+        for k in range(count):
+            j, cp = send(k)
+
+            @pl.when(j != me)
+            def _():
+                cp.wait_send()
+
+    for k in range(1, xc):
+        for cp in held_x(k):
+            cp.wait_send()
+    for xb in range(xc):
+        for cp in held_core(xb):
+            cp.wait_send()
+
+    @pl.loop(0, nz)
+    def _(p):
+        @pl.when((p <= z) & (z < nz - 1))
+        def _():
+            a_z(p, True).wait_send()
+
+        @pl.when((p >= z) & (z > 0))
+        def _():
+            a_z(p, False).wait_send()
+
+        for k in range(1, xc):
+            a_x(p, k).wait_send()
+            r_x(p, k).wait_send()
+        for xb in range(xc):
+            a_core(p, xb).wait_send()
+        r_core(p).wait_send()
+
+        @pl.when(p != z)
+        def _():
+            r_z(p).wait_send()
+
+    for cp in outs:
+        cp.wait()
+
+
+def kernel_plan(
     tokens,
     route_ids,
     route_scores,
@@ -125,86 +641,102 @@
     shared_up,
     shared_down,
 ):
-    fs_count = lax.axis_size("fs")
-    tp_count = lax.axis_size("tp")
-    experts = fs_count * tp_count
-    both = ("fs", "tp")
-    rows_dev, width = tokens.shape
+    nz = lax.axis_size("fs")
+    nt = lax.axis_size("tp")
+    n = nz * nt
+    xc = nt // CORES
+    rows, width = tokens.shape
     widened = tokens.astype(jnp.float32)
     normed = (
         widened * lax.rsqrt(jnp.mean(widened * widened, axis=1, keepdims=True) + EPSILON)
     ).astype(jnp.bfloat16)
     weights = route_scale * route_scores / jnp.sum(route_scores, axis=1, keepdims=True)
-    named = route_ids[:, :, None] == jnp.arange(experts, dtype=jnp.int32)[None, None, :]
-    shares = jnp.sum(jnp.where(named, weights[:, :, None], 0.0), axis=1)
-    gain_col = norm_gain[:, None]
-    cols = expert_gate.shape[2]
-    shared_cols = shared_gate.shape[1]
-    lanes = 2 * shared_cols
-    tile_pair = jnp.concatenate([gain_col * shared_gate, gain_col * shared_up], axis=1).astype(
-        jnp.bfloat16
-    )
-    pair_rows = tile_pair.shape[0]
-    down_rows, down_cols = shared_down.shape
-    strips = down_cols // lanes
-    tile_down = jnp.transpose(
-        shared_down.astype(jnp.bfloat16).reshape(down_rows, strips, lanes), (1, 0, 2)
-    ).reshape(strips * down_rows, lanes)
-    tiles = lax.all_gather(jnp.concatenate([tile_pair, tile_down], axis=0), both, axis=0, tiled=False)
-    tiles = tiles.reshape(fs_count, tp_count, pair_rows + strips * down_rows, lanes)
-    whole_gate = jnp.transpose(tiles[:, :, :pair_rows, :shared_cols], (0, 2, 1, 3)).reshape(
-        fs_count * pair_rows, tp_count * shared_cols
-    )
-    whole_up = jnp.transpose(tiles[:, :, :pair_rows, shared_cols:], (0, 2, 1, 3)).reshape(
-        fs_count * pair_rows, tp_count * shared_cols
-    )
-    whole_down = jnp.transpose(
-        tiles[:, :, pair_rows:].reshape(fs_count, tp_count, strips, down_rows, lanes),
-        (0, 3, 1, 2, 4),
-    ).reshape(fs_count * down_rows, tp_count * down_cols)
-    place = lax.axis_index("fs")
-    held_gate = lax.dynamic_slice_in_dim(whole_gate, place * pair_rows, pair_rows, 0)
-    held_up = lax.dynamic_slice_in_dim(whole_up, place * pair_rows, pair_rows, 0)
-    held_down = lax.dynamic_slice_in_dim(whole_down, place * down_rows, down_rows, 0)
-
-    all_normed = lax.all_gather(
-        lax.all_gather(normed, "fs", axis=0, tiled=True), "tp", axis=0, tiled=True
-    )
-    own_share = lax.all_to_all(
-        shares.T.reshape(experts, 1, rows_dev), both, split_axis=0, concat_axis=1, tiled=True
-    ).reshape(fs_count, tp_count, rows_dev)
-    own_share = jnp.transpose(own_share, (1, 0, 2)).reshape(-1)
-
-    piece_gate = (gain_col[None] * expert_gate).astype(jnp.bfloat16)
-    piece_up = (gain_col[None] * expert_up).astype(jnp.bfloat16)
-    piece_pair = jnp.concatenate([piece_gate, piece_up], axis=2)
-    piece_down = expert_down.astype(jnp.bfloat16)
-    pair = lax.all_to_all(piece_pair[:, None], both, split_axis=0, concat_axis=1, tiled=True)
-    down = lax.all_to_all(piece_down[:, None], both, split_axis=0, concat_axis=1, tiled=True)
-    served_gate = relayout(pair[:, :, :, :cols], fs_count, tp_count)
-    served_up = relayout(pair[:, :, :, cols:], fs_count, tp_count)
-    served_down = relayout(down, fs_count, tp_count)
-    gate_rows = jnp.dot(all_normed, served_gate[0], preferred_element_type=jnp.float32)
-    up_rows = jnp.dot(all_normed, served_up[0], preferred_element_type=jnp.float32)
-    hidden = (jax.nn.silu(gate_rows) * up_rows).astype(jnp.bfloat16)
-    produced = jnp.dot(hidden, served_down[0], preferred_element_type=jnp.float32)
-    partial = (produced * own_share[:, None]).astype(jnp.bfloat16)
-    routed = lax.psum_scatter(partial, "tp", scatter_dimension=0, tiled=True)
-    routed = lax.psum_scatter(routed, "fs", scatter_dimension=0, tiled=True)
-
-    gate_part = jnp.dot(normed, whole_gate, preferred_element_type=jnp.float32)
-    up_part = jnp.dot(normed, whole_up, preferred_element_type=jnp.float32)
-    shared_hidden = (jax.nn.silu(gate_part) * up_part).astype(jnp.bfloat16)
-    shared_term = jnp.dot(shared_hidden, whole_down, preferred_element_type=jnp.float32)
-    mixed = (routed.astype(jnp.float32) + shared_term).astype(jnp.bfloat16)
-    return (mixed, served_gate, served_up, served_down, held_gate, held_up, held_down)
+    named = route_ids.T[None, :, :] == jnp.arange(n, dtype=jnp.int32)[:, None, None]
+    shares = jnp.sum(jnp.where(named, weights.T[None], 0.0), axis=1)[:, None, :]
+    gu = jnp.stack(
+        [
+            (norm_gain * jnp.swapaxes(expert_gate, 1, 2)).astype(jnp.bfloat16),
+            (norm_gain * jnp.swapaxes(expert_up, 1, 2)).astype(jnp.bfloat16),
+        ],
+        axis=1,
+    )
+    dn = expert_down.astype(jnp.bfloat16)
+    sgu = jnp.stack(
+        [
+            (norm_gain * shared_gate.T).astype(jnp.bfloat16),
+            (norm_gain * shared_up.T).astype(jnp.bfloat16),
+        ],
+        axis=0,
+    )
+    sdn = shared_down.astype(jnp.bfloat16)
+    ft, dt = gu.shape[2], gu.shape[3]
+    fr, dc = dn.shape[1], dn.shape[2]
+    inner = ft * nt
+    sd = sgu.shape[1] * nt // n
+    bf = jnp.bfloat16
+    dma = pltpu.SemaphoreType.DMA
+    hbm = pl.BlockSpec(memory_space=pltpu.HBM)
+    mixed, wall, hgu, hd = pl.pallas_call(
+        functools.partial(handover_kernel, nz, nt),
+        out_shape=(
+            jax.ShapeDtypeStruct((rows, width), bf),
+            jax.ShapeDtypeStruct((3, inner, width), bf),
+            jax.ShapeDtypeStruct((2, sgu.shape[1] * nt, dt), bf),
+            jax.ShapeDtypeStruct((sdn.shape[0], width), bf),
+        ),
+        in_specs=[hbm] * 6,
+        out_specs=(hbm,) * 4,
+        scratch_shapes=[
+            pltpu.VMEM((3, inner + sd, width), bf),
+            pltpu.VMEM((n, rows, width), bf),
+            pltpu.VMEM((n, rows, width), bf),
+            pltpu.VMEM((nz * xc, rows, width), bf),
+            pltpu.VMEM((nz * (xc - 1), rows, width), bf),
+            pltpu.VMEM((nz, rows, width), bf),
+            pltpu.VMEM((n, 1, rows), jnp.float32),
+            pltpu.VMEM((2, sgu.shape[1] * nt, dt), bf),
+            pltpu.VMEM((sdn.shape[0], width), bf),
+            pltpu.VMEM((rows, width), bf),
+            dma((8,)),
+            dma((2, n)),
+            dma((2, n)),
+            dma((2, n)),
+            dma((2, n)),
+            dma((n,)),
+            dma((n,)),
+            dma((2, max(nz, nt))),
+            dma((2, max(nz, nt))),
+            dma((4, xc)),
+            dma((2, nt)),
+            dma((2 + xc, n)),
+            dma((n,)),
+            dma((nz,)),
+            dma((nz,)),
+            dma((nz, xc)),
+            dma((nz, xc)),
+            dma((nz,)),
+            dma((nz,)),
+        ],
+        compiler_params=pltpu.CompilerParams(
+            collective_id=0, has_side_effects=True, vmem_limit_bytes=60 << 20
+        ),
+    )(normed, gu, dn, sgu, sdn, shares)
+    return (
+        mixed,
+        wall[0].T[None],
+        wall[1].T[None],
+        wall[2][None],
+        hgu[0].T,
+        hgu[1].T,
+        hd,
+    )
 
 
 def on_device(*args):
     experts = lax.axis_size("fs") * lax.axis_size("tp")
     picks = args[1].shape[1]
     if experts <= 4 * picks:
-        return dense_plan(*args)
+        return kernel_plan(*args)
     return dispatch_plan(*args)
 
 

time: 314 us -> 216 us (0.69)
  waiting for transfers between devices: 209 us -> 0 us
  Pallas kernels: 0 us -> 190 us
  local copies, waits for them, and re-layouts: 38.8 us -> 9.97 us
  matrix products: 24.7 us -> 0 us
  between operations: 15.5 us -> 0.68 us
  starting transfers between devices: 14.4 us -> 0 us
  other arithmetic: 10.4 us -> 14.3 us
    pallas_call x0 -> x1, Pallas kernels: none -> 190 us  [kernel_plan(): pl.pallas_call(functools.partial(handover_kernel, nz, nt), out_shape=(jax...]
    reduce_scatter x2 -> x0, waiting for transfers between devices: 95.7 us -> none  [the longest x1 81.5 us: dense_plan(): routed = lax.psum_scatter(partial, 'tp', scatter_dimension=0, tiled=True)]
    all_to_all x3 -> x0, waiting for transfers between devices: 62.1 us -> none  [the longest x1 37.7 us: dense_plan(): lax.all_to_all(piece_pair[:, None], both, split_axis=0, concat_axis=1, ti...]
    all_gather x3 -> x0, waiting for transfers between devices: 51.5 us -> none  [the longest x1 48.5 us: dense_plan(): lax.all_gather(normed, 'fs', axis=0, tiled=True)]
    dot_general x4 -> x0, matrix products: 24.7 us -> none  [the longest x1 13.8 us: dense_plan(): jnp.dot(hidden, served_down[0], preferred_element_type=jnp.float32)]
    all_to_all x3 -> x0, starting transfers between devices: 14 us -> none  [the longest x1 6.84 us: dense_plan(): lax.all_to_all(piece_pair[:, None], both, split_axis=0, concat_axis=1, ti...]
    transpose x6 -> x1, local copies, waits for them, and re-layouts: 11.1 us -> 1.07 us  [kernel_plan(): hgu[1]]
    reshape x9 -> x0, local copies, waits for them, and re-layouts: 8.88 us -> none  [the longest x3 3.67 us: relayout(): grid = arrived.reshape(fs_count, tp_count, tile_rows, tile_cols)]
  transfers between devices with their start and end apart: 8 -> 0, of which waited for: 7 -> 0; matrix products, arithmetic and copies ran while one was open for 15% -> 0% of each run, Pallas kernels for 0% -> 0%
where the time goes in v1:
time: 216 us; the launch traced here: 215 us
  Pallas kernels  190 us (88%)
  other arithmetic  14.3 us (7%)
  local copies, waits for them, and re-layouts  9.97 us (5%)
    pallas_call x1, Pallas kernels, kernel_plan(): pl.pallas_call(functools.partial(handover_kernel, nz, nt), out_shape=(jax...  190 us
    unnamed x16, local copies, waits for them, and re-layouts  5.79 us

profile of v1, /device:TPU:0, one launch (start us, length us, event | category | flops | bytes accessed | tf_op | source)
XLA Modules:
  0.0 215.2 jit_solution(10186219068949929024)
XLA Ops:
  0.6 0.0 copy-start
  0.6 1.4 fusion
  2.0 0.7 reduce_sum.28
  2.7 0.7 divide_bitcast_fusion
  3.4 1.3 select_reduce_fusion
  4.7 1.5 convert_element_type.47.sdn
  6.3 1.0 fusion.4
  7.3 0.7 pad_maximum_fusion.1.sgu
  8.0 0.0 copy-start.1
  8.0 0.0 copy-start.4
  8.0 2.1 fusion.1.normed
  10.1 0.0 copy-done
  10.1 1.1 convert_element_type.42.dn
  11.2 0.0 copy-done.1
  11.2 0.0 copy-done.4
  11.2 2.2 %fusion.2 = (bf16[16,1,64,512]{3,2,1,0:T(8,128)(2,1)S(1)}, bf16[16,1,64,512]{3,2,1,0:T(8,128)(2,1)S(1)}) fusion(f32[16,512,64]{1,2,0:T(8,128)S(1)} %copy-done.1, f32[512]{0:T(512)S(1)} %copy-done.4, f32[16,512,64]{1,2,0:T(8,128)} %param.15), kind=kLoop, calls=%fused_computation.7 | loop fusion | flops 2097152 | bytes 6293504 | tf_op jit(solution)/shard_map/stack | solution.py:656
  13.4 1.5 pad_maximum_fusion.gu
  15.0 190.2 %shard_map.153 = (bf16[128,2048]{1,0:T(8,128)(2,1)}, bf16[3,256,2048]{2,1,0:T(8,128)(2,1)}, bf16[2,256,512]{2,1,0:T(8,128)(2,1)}, bf16[64,2048]{1,0:T(8,128)(2,1)}) custom-call(bf16[128,2048]{1,0:T(8,128)(2,1)} %fusion.1.normed, bf16[16,2,64,512]{3,2,1,0:T(8,128)(2,1)} %pad_maximum_fusion.gu, bf16[16,64,512]{2,1,0:T(8,128)(2,1)} %convert_element_type.42.dn, ...), custom_call_target="tpu_custom_call" | custom-call | tf_op jit(solution)/shard_map/pallas_call | solution.py:679
  205.2 1.1 slice_bitcast_fusion.2
  206.3 0.8 copy.26
  207.1 0.8 copy.25
  208.0 3.1 %fusion.6 = (bf16[1,256,2048]{2,1,0:T(8,128)(2,1)}, bf16[1,2048,256]{1,2,0:T(8,128)(2,1)S(1)}, bf16[1,2048,256]{1,2,0:T(8,128)(2,1)S(1)}) fusion(bf16[3,256,2048]{2,1,0:T(8,128)(2,1)} %get-tuple-element.12), kind=kLoop, calls=%fused_computation.22 | loop fusion | bytes 6291456 | tf_op jit(solution)/shard_map/slice | solution.py:728
  211.1 0.0 copy-start.2
  211.1 1.3 copy.24
  212.4 0.0 copy-start.3
  212.4 1.3 copy.23
  213.7 0.0 copy-done.2
  213.7 0.8 copy.29
  214.5 0.0 copy-done.3
  214.5 0.7 copy.30
  (1 shorter events, 0.0 us)
Async XLA Ops:
  0.6 9.5 %copy-start = (f32[16,64,512]{2,1,0:T(8,128)S(1)}, f32[16,64,512]{2,1,0:T(8,128)}, u32[]{:S(2)}) copy-start(f32[16,64,512]{2,1,0:T(8,128)} %param.16) | copy-start | bytes 6291460
  8.0 3.3 %copy-start.1 = (f32[16,512,64]{1,2,0:T(8,128)S(1)}, f32[16,512,64]{1,2,0:T(8,128)}, u32[]{:S(2)}) copy-start(f32[16,512,64]{1,2,0:T(8,128)} %param.14) | copy-start | bytes 6291460
  8.0 3.3 %copy-start.4 = (f32[512]{0:T(512)S(1)}, f32[512]{0:T(512)}, u32[]{:S(2)}) copy-start(f32[512]{0:T(512)} %param.13) | copy-start | bytes 6148
  211.1 2.6 %copy-start.2 = (bf16[128,2048]{1,0:T(8,128)(2,1)S(1)}, bf16[128,2048]{1,0:T(8,128)(2,1)}, u32[]{:S(2)}) copy-start(bf16[128,2048]{1,0:T(8,128)(2,1)} %get-tuple-element.45) | copy-start | bytes 1572868
  212.4 2.1 copy-start.3

commit v2 on v1

v2 whole, which is shorter than its diff:
```python
import functools
import jax
import jax.numpy as jnp
from jax import lax
from jax.experimental import pallas as pl
from jax.experimental.pallas import tpu as pltpu
from jax.sharding import PartitionSpec as P

EPSILON = 1e-06
route_scale = 2.5
CORES = 2
MESH = pl.DeviceIdType.MESH


def expert_rows(row_block, w_gate, w_up, w_down):
    gate_rows = jnp.dot(row_block, w_gate, preferred_element_type=jnp.float32)
    up_rows = jnp.dot(row_block, w_up, preferred_element_type=jnp.float32)
    hidden = (jax.nn.silu(gate_rows) * up_rows).astype(jnp.bfloat16)
    return jnp.dot(hidden, w_down, preferred_element_type=jnp.float32).astype(jnp.bfloat16)


def relayout(arrived, fs_count, tp_count):
    tile_rows = arrived.shape[2]
    tile_cols = arrived.shape[3]
    grid = arrived.reshape(fs_count, tp_count, tile_rows, tile_cols)
    grid = jnp.transpose(grid, (0, 2, 1, 3))
    return grid.reshape(1, fs_count * tile_rows, tp_count * tile_cols)


def dispatch_plan(
    tokens,
    route_ids,
    route_scores,
    norm_gain,
    expert_gate,
    expert_up,
    expert_down,
    shared_gate,
    shared_up,
    shared_down,
):
    fs_count = lax.axis_size("fs")
    tp_count = lax.axis_size("tp")
    experts = fs_count * tp_count
    gain_col = norm_gain[:, None]
    piece_gate = (gain_col[None] * expert_gate).astype(jnp.bfloat16)
    piece_up = (gain_col[None] * expert_up).astype(jnp.bfloat16)
    piece_down = expert_down.astype(jnp.bfloat16)
    moved = (
        lax.all_to_all(piece_gate[:, None], ("fs", "tp"), split_axis=0, concat_axis=1, tiled=True),
        lax.all_to_all(piece_up[:, None], ("fs", "tp"), split_axis=0, concat_axis=1, tiled=True),
        lax.all_to_all(piece_down[:, None], ("fs", "tp"), split_axis=0, concat_axis=1, tiled=True),
    )
    served_gate = relayout(moved[0], fs_count, tp_count)
    served_up = relayout(moved[1], fs_count, tp_count)
    served_down = relayout(moved[2], fs_count, tp_count)
    tile_gate = (gain_col * shared_gate).astype(jnp.bfloat16)
    tile_up = (gain_col * shared_up).astype(jnp.bfloat16)
    tile_down = shared_down.astype(jnp.bfloat16)
    held_gate, held_up, held_down = (
        lax.all_gather(tile_gate, "tp", axis=1, tiled=True),
        lax.all_gather(tile_up, "tp", axis=1, tiled=True),
        lax.all_gather(tile_down, "tp", axis=1, tiled=True),
    )
    rows_dev = tokens.shape[0]
    width = tokens.shape[1]
    picks = route_ids.shape[1]
    capacity = 3 * rows_dev * picks // (2 * experts)
    widened = tokens.astype(jnp.float32)
    normed = (
        widened * lax.rsqrt(jnp.mean(widened * widened, axis=1, keepdims=True) + EPSILON)
    ).astype(jnp.bfloat16)
    weights = route_scale * route_scores / jnp.sum(route_scores, axis=1, keepdims=True)
    flat_ids = route_ids.reshape(-1)
    onehot = (flat_ids[:, None] == jnp.arange(experts, dtype=jnp.int32)[None, :]).astype(jnp.int32)
    earlier = jnp.cumsum(onehot, axis=0) - onehot
    ranks = jnp.sum(earlier * onehot, axis=1)
    target = flat_ids * capacity + ranks
    outbox = (
        jnp.zeros((experts * capacity, width), jnp.bfloat16)
        .at[target]
        .set(jnp.repeat(normed, picks, axis=0))
    )
    arrived = lax.all_to_all(
        outbox.reshape(experts, capacity, width),
        ("fs", "tp"),
        split_axis=0,
        concat_axis=0,
        tiled=True,
    )
    finished = expert_rows(
        arrived.reshape(-1, width), served_gate[0], served_up[0], served_down[0]
    ).reshape(arrived.shape)
    returned = lax.all_to_all(finished, ("fs", "tp"), split_axis=0, concat_axis=0, tiled=True)
    results = returned.reshape(experts * capacity, width)[target]
    routed = jnp.sum(
        results.reshape(rows_dev, picks, width).astype(jnp.float32) * weights[:, :, None], axis=1
    )
    columns = normed
    gate_part = jnp.dot(
        columns,
        lax.all_gather(held_gate, "fs", axis=0, tiled=True),
        preferred_element_type=jnp.float32,
    )
    up_part = jnp.dot(
        columns,
        lax.all_gather(held_up, "fs", axis=0, tiled=True),
        preferred_element_type=jnp.float32,
    )
    shared_hidden = (jax.nn.silu(gate_part) * up_part).astype(jnp.bfloat16)
    columns = shared_hidden
    shared_term = jnp.dot(
        columns,
        lax.all_gather(held_down, "fs", axis=0, tiled=True),
        preferred_element_type=jnp.float32,
    )
    mixed = (routed + shared_term).astype(jnp.bfloat16)
    return (mixed, served_gate, served_up, served_down, held_gate, held_up, held_down)


def handover_kernel(
    nz,
    nt,
    tokens,
    ids,
    scores,
    gain,
    in_gate,
    in_up,
    in_down,
    in_sgate,
    in_sup,
    in_sdown,
    o_mix,
    o_gate,
    o_up,
    o_down,
    o_hgate,
    o_hup,
    o_hd,
    l_tok,
    l_ids,
    l_scores,
    l_gain,
    l_gate,
    l_up,
    l_down,
    l_sgate,
    l_sup,
    l_sdown,
    gu,
    dn,
    sgu,
    sdn,
    shares,
    w,
    tok,
    part,
    rd,
    rx,
    rz,
    ry,
    total,
    share,
    hgu,
    hd,
    flip,
    hflip,
    lsem,
    osem,
    wsend,
    wrecv,
    ysend,
    yrecv,
    shsend,
    shrecv,
    ssend,
    srecv,
    hsend,
    hrecv,
    asend,
    arecv,
    rdsend,
    rdrecv,
    rxsend,
    rxrecv,
    rzsend,
    rzrecv,
    ryrecv,
):
    n = nz * nt
    xc = nt // CORES
    g = lax.axis_index("grp")
    z = lax.axis_index("fs")
    t = lax.axis_index("tp")
    x = t // CORES
    c = t % CORES
    me = z * nt + t
    rows, width = tokens.shape
    ft, dt = in_gate.shape[1], in_gate.shape[2]
    fr, dc = in_down.shape[1], in_down.shape[2]
    st, sr = in_sgate.shape[0], in_sdown.shape[0]
    inner = ft * nt
    sd = w.shape[1] - inner
    half_f, half_r, half_st, half_sr = ft // 2, fr // 2, st // 2, sr // 2

    def dev(zz, tt, gg=None):
        return {"grp": g if gg is None else gg, "fs": zz, "tp": tt}

    def rem(src, dst, ssem, rsem, device):
        return pltpu.make_async_remote_copy(
            src_ref=src,
            dst_ref=dst,
            send_sem=ssem,
            recv_sem=rsem,
            device_id=device,
            device_id_type=MESH,
        )

    def al(v, m):
        return pl.multiple_of(v, m)

    partner = dev(z, x * CORES + 1 - c)
    across = dev(z, t, 1 - g)
    mate = z * nt + x * CORES + 1 - c

    def xdev(k):
        return dev(z, lax.rem(x + k, xc) * CORES + c)

    def slot(p, h, xb):
        return p * nt + h * xc + xb

    own = slot(z, c, x)

    barrier = pltpu.get_barrier_semaphore()

    @pl.loop(1, n)
    def _(k):
        j = lax.rem(me + k, n)
        pl.semaphore_signal(barrier, 1, device_id=dev(j // nt, j % nt), device_id_type=MESH)

    pl.semaphore_signal(barrier, 1, device_id=across, device_id_type=MESH)

    loads = [
        pltpu.make_async_copy(src, dst, lsem.at[i])
        for i, (src, dst) in enumerate(
            (
                (tokens, l_tok),
                (gain, l_gain),
                (in_gate, l_gate),
                (in_up, l_up),
                (in_down, l_down),
                (in_sgate, l_sgate),
                (in_sup, l_sup),
                (in_sdown, l_sdown),
                (ids, l_ids),
                (scores, l_scores),
            )
        )
    ]
    for cp in loads:
        cp.start()
    loads[0].wait()
    band = min(32, rows)

    @pl.loop(0, rows // band)
    def _(r):
        at = pl.ds(al(r * band, band), band)
        wide = l_tok[at, :].astype(jnp.float32)
        mean = jnp.mean(wide * wide, axis=1, keepdims=True)
        tok[own, at, :] = (wide * lax.rsqrt(mean + EPSILON)).astype(jnp.bfloat16)

    for cp in loads[1:]:
        cp.wait()

    @pl.loop(0, n)
    def _(e):
        gu[e, 0] = (l_gain[...] * l_gate[e]).astype(jnp.bfloat16)
        gu[e, 1] = (l_gain[...] * l_up[e]).astype(jnp.bfloat16)
        dn[e] = l_down[e].astype(jnp.bfloat16)

    sgu[0] = (l_gain[...] * l_sgate[...]).astype(jnp.bfloat16)
    sgu[1] = (l_gain[...] * l_sup[...]).astype(jnp.bfloat16)
    sdn[...] = l_sdown[...].astype(jnp.bfloat16)
    sc = l_scores[...]
    mixing = route_scale * sc / jnp.sum(sc, axis=0, keepdims=True)
    for e in range(n):
        shares[e] = jnp.sum(jnp.where(l_ids[...] == e, mixing, 0.0), axis=0, keepdims=True)
    own_gu = (pl.ds(0, 2), pl.ds(al(t * ft, ft), ft), pl.ds(al(z * dt, dt), dt))
    w[own_gu] = gu[me]
    w[2, pl.ds(al(z * fr, fr), fr), pl.ds(al(t * dc, dc), dc)] = dn[me]
    hgu[:, pl.ds(al(t * st, st), st), :] = sgu[...]
    hd[:, pl.ds(al(t * dc, dc), dc)] = sdn[...]
    share[me] = shares[me]

    @pl.when(me // nz == t)
    def _():
        w[pl.ds(0, 2), pl.ds(inner, sd), pl.ds(al(z * dt, dt), dt)] = sgu[
            :, pl.ds(al((me % nz) * sd, sd), sd), :
        ]

    @pl.when(me // nt == z)
    def _():
        w[2, pl.ds(inner, sd), pl.ds(al(t * dc, dc), dc)] = sdn[
            pl.ds(al((me % nt) * sd, sd), sd), :
        ]

    pl.semaphore_wait(barrier, n)

    def gu_at(src, gg):
        zs, ts = src // nt, src % nt
        return w.at[
            pl.ds(0, 2), pl.ds(al(ts * ft + gg * half_f, half_f), half_f), pl.ds(al(zs * dt, dt), dt)
        ]

    def dn_at(src, gg):
        zs, ts = src // nt, src % nt
        return w.at[2, pl.ds(al(zs * fr + gg * half_r, half_r), half_r), pl.ds(al(ts * dc, dc), dc)]

    def w_send(j, gg, ssem, rsem):
        device = dev(j // nt, j % nt)
        return (
            rem(
                gu.at[j, pl.ds(0, 2), pl.ds(al(gg * half_f, half_f), half_f), :],
                gu_at(me, gg),
                ssem.at[0, j],
                rsem.at[0, me],
                device,
            ),
            rem(
                dn.at[j, pl.ds(al(gg * half_r, half_r), half_r), :],
                dn_at(me, gg),
                ssem.at[1, j],
                rsem.at[1, me],
                device,
            ),
        )

    def w_out(j):
        return w_send(j, g, wsend, wrecv)

    def w_mate():
        return w_send(mate, 1 - g, ysend, yrecv)

    def w_across(s, gg):
        return (
            rem(gu_at(s, gg), gu_at(s, gg), ysend.at[0, s], yrecv.at[0, s], across),
            rem(dn_at(s, gg), dn_at(s, gg), ysend.at[1, s], yrecv.at[1, s], across),
        )

    def w_plane_send(p):
        @pl.loop(0, nt)
        def _(tt):
            for cp in w_out(p * nt + tt):
                cp.start()

    def w_plane_across(p):
        @pl.loop(0, nt)
        def _(tt):
            s = p * nt + tt
            for i, at in ((0, gu_at), (1, dn_at)):
                rem(at(s, g), at(s, g), ysend.at[i, s], wrecv.at[i, s], across).wait_recv()
            for cp in w_across(s, g):
                cp.start()

    def share_send(j):
        return rem(shares.at[j], share.at[me], shsend.at[j], shrecv.at[me], dev(j // nt, j % nt))

    def sgu_at(zs):
        return w.at[pl.ds(0, 2), pl.ds(inner, sd), pl.ds(al(zs * dt, dt), dt)]

    def sdn_at(ts):
        return w.at[2, pl.ds(inner, sd), pl.ds(al(ts * dc, dc), dc)]

    def sgu_send(k):
        j = t * nz + k
        return j, rem(
            sgu.at[pl.ds(0, 2), pl.ds(k * sd, sd), :],
            sgu_at(z),
            ssend.at[0, k],
            srecv.at[0, z],
            dev(j // nt, j % nt),
        )

    def sdn_send(k):
        j = z * nt + k
        return j, rem(
            sdn.at[pl.ds(k * sd, sd), :],
            sdn_at(t),
            ssend.at[1, k],
            srecv.at[1, t],
            dev(j // nt, j % nt),
        )

    def hgu_half(ts, gg):
        return hgu.at[pl.ds(0, 2), pl.ds(al(ts * st + gg * half_st, half_st), half_st), :]

    def hd_half(ts, gg):
        return hd.at[pl.ds(al(gg * half_sr, half_sr), half_sr), pl.ds(al(ts * dc, dc), dc)]

    def hgu_at(ts):
        return hgu.at[pl.ds(0, 2), pl.ds(al(ts * st, st), st), :]

    def hd_at(ts):
        return hd.at[:, pl.ds(al(ts * dc, dc), dc)]

    def held_x(k):
        return (
            rem(
                sgu.at[pl.ds(0, 2), pl.ds(al(g * half_st, half_st), half_st), :],
                hgu_half(t, g),
                hsend.at[0, t],
                hrecv.at[0, t],
                xdev(k),
            ),
            rem(
                sdn.at[pl.ds(al(g * half_sr, half_sr), half_sr), :],
                hd_half(t, g),
                hsend.at[1, t],
                hrecv.at[1, t],
                xdev(k),
            ),
        )

    def held_x_in(ts):
        return (
            rem(hgu_half(ts, g), hgu_half(ts, g), hsend.at[0, ts], hrecv.at[0, ts], across),
            rem(hd_half(ts, g), hd_half(ts, g), hsend.at[1, ts], hrecv.at[1, ts], across),
        )

    def held_across(ts, gg):
        return (
            rem(hgu_half(ts, gg), hgu_half(ts, gg), hsend.at[2, ts], hrecv.at[2, ts], across),
            rem(hd_half(ts, gg), hd_half(ts, gg), hsend.at[3, ts], hrecv.at[3, ts], across),
        )

    def held_core(ts):
        return (
            rem(hgu_at(ts), hgu_at(ts), hsend.at[4, ts], hrecv.at[4, ts], partner),
            rem(hd_at(ts), hd_at(ts), hsend.at[5, ts], hrecv.at[5, ts], partner),
        )

    def a_z(p, up):
        s = slot(p, c, x)
        return rem(
            tok.at[s],
            tok.at[s],
            asend.at[0 if up else 1, s],
            arecv.at[s],
            dev(z + 1 if up else z - 1, t),
        )

    def a_x(p, k):
        s = slot(p, c, x)
        return rem(tok.at[s], tok.at[s], asend.at[2 + k, s], arecv.at[s], xdev(k))

    def a_core(p, xb):
        s = slot(p, c, xb)
        return rem(tok.at[s], tok.at[s], asend.at[2, s], arecv.at[s], partner)

    def a_wait(s):
        rem(tok.at[s], tok.at[s], asend.at[2, s], arecv.at[s], partner).wait_recv()

    def a_cross(p):
        for k in range(1, xc):
            xb = lax.rem(x + k, xc)
            a_wait(slot(p, c, xb))
            a_core(p, xb).start()

    def r_core(p):
        return rem(
            part.at[pl.ds(slot(p, 1 - c, 0), xc)],
            rd.at[pl.ds(p * xc, xc)],
            rdsend.at[p],
            rdrecv.at[p],
            partner,
        )

    def r_x(p, k):
        xb = lax.rem(x + k, xc)
        return rem(
            part.at[slot(p, c, xb)],
            rx.at[p * (xc - 1) + k - 1],
            rxsend.at[p, k - 1],
            rxrecv.at[p, k - 1],
            xdev(k),
        )

    def r_z(p):
        return rem(part.at[slot(p, c, x)], rz.at[z], rzsend.at[p], rzrecv.at[z], dev(p, t))

    near = jnp.where(z == 0, 1, nz - 2)

    def r_relay(p):
        return rem(part.at[slot(p, c, x)], ry.at[p], rzsend.at[p], ryrecv.at[p], dev(near, t))

    def relayed(p):
        return ((z == 1) & (p > 1)) | ((z == nz - 2) & (p < nz - 2))

    @pl.loop(1, nt)
    def _(k):
        for cp in w_out(z * nt + lax.rem(t + k, nt)):
            cp.start()

    for cp in w_mate():
        cp.start()

    @pl.when(z < nz - 1)
    def _():
        a_z(z, True).start()

    @pl.when(z > 0)
    def _():
        a_z(z, False).start()

    a_core(z, x).start()
    for k in range(1, xc):
        a_x(z, k).start()

    @pl.loop(1, n)
    def _(k):
        share_send(lax.rem(me + k, n)).start()

    def send_when(j, cp):
        @pl.when(j != me)
        def _():
            cp.start()

    last = jnp.where(2 * z < nz, nz - 1 - z, z)

    edge = (z == 0) | (z == nz - 1)

    @pl.loop(0, nz + 1)
    def _(d):
        late = edge & (d == nz - 1)

        @pl.when((d > 0) & (z - d >= 0) & ~late)
        def _():
            p = z - d
            a_wait(slot(p, c, x))

            @pl.when(z < nz - 1)
            def _():
                a_z(p, True).start()

            for k in range(1, xc):
                a_x(p, k).start()
            a_core(p, x).start()

        @pl.when((d > 0) & (z + d < nz) & ~late)
        def _():
            p = z + d
            a_wait(slot(p, c, x))

            @pl.when(z > 0)
            def _():
                a_z(p, False).start()

            for k in range(1, xc):
                a_x(p, k).start()
            a_core(p, x).start()

        @pl.when(d == nz - 1)
        def _():
            for send, count in ((sgu_send, nz), (sdn_send, nt)):
                for k in range(count):
                    send_when(*send(k))

            for k in range(1, xc):
                for cp in held_x(k):
                    cp.start()

        @pl.when(d < nz)
        def _():
            stop = jnp.where(edge | (d < last), d, nz - 1)

            @pl.loop(d, stop + 1)
            def _(q):
                @pl.when((q > z) & (edge | (d <= last)))
                def _():
                    w_plane_send(q)

                @pl.when((nz - 1 - q < z) & (edge | (d <= last)))
                def _():
                    w_plane_send(nz - 1 - q)

        @pl.when(d == 1)
        def _():
            @pl.loop(1, nt)
            def _(k):
                s = z * nt + lax.rem(t + k, nt)
                for i, at in ((0, gu_at), (1, dn_at)):
                    rem(at(s, g), at(s, g), ysend.at[i, s], wrecv.at[i, s], across).wait_recv()

                @pl.when(s != mate)
                def _():
                    for cp in w_across(s, g):
                        cp.start()

        @pl.when(late)
        def _():
            p = nz - 1 - z
            w_plane_across(p)
            a_wait(slot(p, c, x))
            for k in range(1, xc):
                a_x(p, k).start()
            a_core(p, x).start()

        @pl.when((d == z + 1) & (z < nz - 1))
        def _():
            @pl.loop(0, z)
            def _(p):
                w_plane_across(p)

        @pl.when((d == nz - z) & (z > 0))
        def _():
            @pl.loop(z + 1, nz)
            def _(k):
                w_plane_across(nz + z - k)

        @pl.when(edge & (d == nz))
        def _():
            @pl.loop(1, nz - 1)
            def _(k):
                w_plane_across(jnp.where(z == 0, nz - 1 - k, k))

    @pl.loop(0, nz)
    def _(k):
        a_cross(lax.rem(z + k, nz))

    for k in range(1, xc):
        ts = lax.rem(x + k, xc) * CORES + c
        for cp in held_x_in(ts):
            cp.wait_recv()
        for cp in held_across(ts, g):
            cp.start()

    @pl.loop(1, n)
    def _(k):
        s = lax.rem(me + n - k, n)
        for cp in w_across(s, 1 - g):
            cp.wait_recv()
        rem(shares.at[s], share.at[s], shsend.at[s], shrecv.at[s], across).wait_recv()

    for k in range(nz):

        @pl.when(k * nt + me // nz != me)
        def _():
            rem(sgu_at(k), sgu_at(k), ssend.at[0, k], srecv.at[0, k], across).wait_recv()

    for k in range(nt):

        @pl.when((me // nt) * nt + k != me)
        def _():
            rem(sdn_at(k), sdn_at(k), ssend.at[1, k], srecv.at[1, k], across).wait_recv()

    out_down = pltpu.make_async_copy(w.at[2, pl.ds(0, inner), :], o_down, osem.at[0])
    out_down.start()
    nt_dims = (((1,), (1,)), ((), ()))

    def compute(p, h):
        first = slot(p, h, 0)
        xs = tok[pl.ds(first, xc)].reshape(xc * rows, width)
        gate = lax.dot_general(xs, w[0], nt_dims, preferred_element_type=jnp.float32)
        up = lax.dot_general(xs, w[1], nt_dims, preferred_element_type=jnp.float32)
        hidden = gate / (1.0 + jnp.exp(-gate)) * up
        scale = jnp.concatenate(
            [
                jnp.transpose(jnp.broadcast_to(share[p * nt + xb * CORES + h], (rows, rows)))
                for xb in range(xc)
            ],
            axis=0,
        )[:, :1]
        col = lax.broadcasted_iota(jnp.int32, hidden.shape, 1)
        hidden = jnp.where(col < inner, hidden * scale, hidden).astype(jnp.bfloat16)
        step = min(512, width)
        for lo in range(0, width, step):
            res = jnp.dot(hidden, w[2, :, lo : lo + step], preferred_element_type=jnp.float32)
            part[pl.ds(first, xc), :, lo : lo + step] = res.astype(jnp.bfloat16).reshape(
                xc, rows, step
            )

    def work(p):
        for xb in range(xc):
            a_wait(slot(p, 1 - c, xb))

        @pl.loop(0, 2)
        def _(j):
            compute(p, (1 - c) * (1 - j) + c * j)

            @pl.when(j == 0)
            def _():
                r_core(p).start()

        r_core(p).wait_recv()
        for k in range(1, xc):
            xb = lax.rem(x + k, xc)
            s = slot(p, c, xb)
            part[s] = (part[s].astype(jnp.float32) + rd[p * xc + xb].astype(jnp.float32)).astype(
                jnp.bfloat16
            )
            r_x(p, k).start()

    def settle(p):
        s = slot(p, c, x)
        acc = part[s].astype(jnp.float32) + rd[p * xc + x].astype(jnp.float32)
        for k in range(1, xc):
            r_x(p, k).wait_recv()
            acc = acc + rx[p * (xc - 1) + k - 1].astype(jnp.float32)
        part[s] = acc.astype(jnp.bfloat16)

        @pl.when(relayed(p))
        def _():
            r_relay(p).wait_recv()
            part[s] = (acc + ry[p].astype(jnp.float32)).astype(jnp.bfloat16)

    low = 2 * z < nz

    def order(i):
        q = jnp.where(edge, i, jnp.where(i == 0, 0, nz - i))
        inside = jnp.where(q == 0, jnp.where(low, 0, nz - 1), jnp.where(low, q, nz - 1 - q))
        ends = jnp.where(low, nz - 1 - i, i)
        return jnp.where(i == nz - 1, z, jnp.where(edge, ends, inside))

    @pl.loop(0, nz)
    def _(i):
        work(order(i))

        @pl.when(i == 0)
        def _():
            for i2 in range(2):
                for lo in range(0, width, 256):
                    flip[i2, lo : lo + 256, :] = jnp.transpose(w[i2, :inner, lo : lo + 256])
            for i2, o_w in enumerate((o_gate, o_up)):
                pltpu.make_async_copy(flip.at[i2], o_w, osem.at[1 + i2]).start()

        @pl.when(i > 0)
        def _():
            p = order(i - 1)
            settle(p)

            @pl.when(edge & (p != near))
            def _():
                r_relay(p).start()

            @pl.when(~edge | (p == near))
            def _():
                r_z(p).start()

    for k in range(1, xc):
        ts = lax.rem(x + k, xc) * CORES + c
        for cp in held_across(ts, 1 - g):
            cp.wait_recv()
    for xb in range(xc):
        for cp in held_core(xb * CORES + c):
            cp.start()
    for xb in range(xc):
        for cp in held_core(xb * CORES + 1 - c):
            cp.wait_recv()
    for i in range(2):
        hflip[i] = jnp.transpose(hgu[i])
    out_held = [
        pltpu.make_async_copy(hflip.at[0], o_hgate, osem.at[3]),
        pltpu.make_async_copy(hflip.at[1], o_hup, osem.at[4]),
        pltpu.make_async_copy(hd, o_hd, osem.at[6]),
    ]
    for cp in out_held:
        cp.start()

    settle(z)
    total[...] = part[own].astype(jnp.float32)
    for k in range(1, nz):
        zs = lax.rem(z + k, nz)

        @pl.when(((zs > 0) & (zs < nz - 1)) | (zs == z + 1) | (zs == z - 1))
        def _():
            rem(rz.at[zs], rz.at[zs], rzsend.at[zs], rzrecv.at[zs], partner).wait_recv()
            total[...] += rz[zs].astype(jnp.float32)

    l_tok[...] = total[...].astype(jnp.bfloat16)
    out_mix = pltpu.make_async_copy(l_tok, o_mix, osem.at[5])
    out_mix.start()

    @pl.loop(1, n)
    def _(k):
        j = lax.rem(me + k, n)
        for cp in w_out(j):
            cp.wait_send()
        share_send(j).wait_send()
        for cp in w_across(j, g):
            cp.wait_send()

    for send, count in ((sgu_send, nz), (sdn_send, nt)):
        for k in range(count):
            j, cp = send(k)

            @pl.when(j != me)
            def _():
                cp.wait_send()

    for k in range(1, xc):
        for cp in held_x(k):
            cp.wait_send()
        for cp in held_across(lax.rem(x + k, xc) * CORES + c, g):
            cp.wait_send()
    for xb in range(xc):
        for cp in held_core(xb * CORES + c):
            cp.wait_send()

    @pl.loop(0, nz)
    def _(p):
        @pl.when((p <= z) & (z < nz - 1))
        def _():
            a_z(p, True).wait_send()

        @pl.when((p >= z) & (z > 0))
        def _():
            a_z(p, False).wait_send()

        for k in range(1, xc):
            a_x(p, k).wait_send()
            r_x(p, k).wait_send()
        for xb in range(xc):
            a_core(p, xb).wait_send()
        r_core(p).wait_send()

        @pl.when(p != z)
        def _():
            r_z(p).wait_send()

    out_down.wait()
    for i, o_w in enumerate((o_gate, o_up)):
        pltpu.make_async_copy(flip.at[i], o_w, osem.at[1 + i]).wait()
    for cp in out_held:
        cp.wait()
    out_mix.wait()


def kernel_plan(
    tokens,
    route_ids,
    route_scores,
    norm_gain,
    expert_gate,
    expert_up,
    expert_down,
    shared_gate,
    shared_up,
    shared_down,
):
    nz = lax.axis_size("fs")
    nt = lax.axis_size("tp")
    n = nz * nt
    xc = nt // CORES
    rows, width = tokens.shape
    picks = route_ids.shape[1]
    dt, ft = expert_gate.shape[1:]
    fr, dc = expert_down.shape[1:]
    st, sr = shared_gate.shape[1], shared_down.shape[0]
    inner = ft * nt
    sd = st * nt // n
    bf, f4 = jnp.bfloat16, jnp.float32
    dma = pltpu.SemaphoreType.DMA
    hbm = pl.BlockSpec(memory_space=pltpu.HBM)
    outs = (
        (rows, width),
        (width, inner),
        (width, inner),
        (inner, width),
        (dt, st * nt),
        (dt, st * nt),
        (sr, width),
    )
    mixed, gate, up, down, hgate, hup, hd = pl.pallas_call(
        functools.partial(handover_kernel, nz, nt),
        out_shape=tuple(jax.ShapeDtypeStruct(s, bf) for s in outs),
        in_specs=[hbm] * 10,
        out_specs=(hbm,) * len(outs),
        scratch_shapes=[
            pltpu.VMEM((rows, width), bf),
            pltpu.VMEM((picks, rows), jnp.int32),
            pltpu.VMEM((picks, rows), f4),
            pltpu.VMEM((1, dt), f4),
            pltpu.VMEM((n, ft, dt), f4),
            pltpu.VMEM((n, ft, dt), f4),
            pltpu.VMEM((n, fr, dc), f4),
            pltpu.VMEM((st, dt), f4),
            pltpu.VMEM((st, dt), f4),
            pltpu.VMEM((sr, dc), f4),
            pltpu.VMEM((n, 2, ft, dt), bf),
            pltpu.VMEM((n, fr, dc), bf),
            pltpu.VMEM((2, st, dt), bf),
            pltpu.VMEM((sr, dc), bf),
            pltpu.VMEM((n, 1, rows), f4),
            pltpu.VMEM((3, inner + sd, width), bf),
            pltpu.VMEM((n, rows, width), bf),
            pltpu.VMEM((n, rows, width), bf),
            pltpu.VMEM((nz * xc, rows, width), bf),
            pltpu.VMEM((nz * (xc - 1), rows, width), bf),
            pltpu.VMEM((nz, rows, width), bf),
            pltpu.VMEM((nz, rows, width), bf),
            pltpu.VMEM((rows, width), f4),
            pltpu.VMEM((n, 1, rows), f4),
            pltpu.VMEM((2, st * nt, dt), bf),
            pltpu.VMEM((sr, width), bf),
            pltpu.VMEM((2, width, inner), bf),
            pltpu.VMEM((2, dt, st * nt), bf),
            dma((10,)),
            dma((7,)),
            dma((2, n)),
            dma((2, n)),
            dma((2, n)),
            dma((2, n)),
            dma((n,)),
            dma((n,)),
            dma((2, max(nz, nt))),
            dma((2, max(nz, nt))),
            dma((6, nt)),
            dma((6, nt)),
            dma((2 + xc, n)),
            dma((n,)),
            dma((nz,)),
            dma((nz,)),
            dma((nz, xc)),
            dma((nz, xc)),
            dma((nz,)),
            dma((nz,)),
            dma((nz,)),
        ],
        compiler_params=pltpu.CompilerParams(
            collective_id=0, has_side_effects=True, vmem_limit_bytes=60 << 20
        ),
    )(
        tokens,
        route_ids.T,
        route_scores.T,
        norm_gain[None],
        jnp.swapaxes(expert_gate, 1, 2),
        jnp.swapaxes(expert_up, 1, 2),
        expert_down,
        shared_gate.T,
        shared_up.T,
        shared_down,
    )
    return mixed, gate[None], up[None], down[None], hgate, hup, hd


def on_device(*args):
    experts = lax.axis_size("fs") * lax.axis_size("tp")
    picks = args[1].shape[1]
    if experts <= 4 * picks:
        return kernel_plan(*args)
    return dispatch_plan(*args)


def solution(mesh):
    return jax.shard_map(
        on_device,
        mesh=mesh,
        in_specs=(
            P(("grp", "fs", "tp"), None),
            P(("grp", "fs", "tp"), None),
            P(("grp", "fs", "tp"), None),
            P("fs"),
            P(None, "fs", "tp"),
            P(None, "fs", "tp"),
            P(None, "fs", "tp"),
            P("fs", "tp"),
            P("fs", "tp"),
            P("fs", "tp"),
        ),
        out_specs=(
            P(("grp", "fs", "tp"), None),
            P(("grp", "fs", "tp"), None, None),
            P(("grp", "fs", "tp"), None, None),
            P(("grp", "fs", "tp"), None, None),
            P(("grp", "fs"), None),
            P(("grp", "fs"), None),
            P(("grp", "fs"), None),
        ),
        check_vma=False,
    )
```

time: 216 us -> 153 us (0.71)
  Pallas kernels: 190 us -> 144 us
  other arithmetic: 14.3 us -> 0 us
    pallas_call x1, Pallas kernels: 190 us -> 144 us  [kernel_plan(): pl.pallas_call(functools.partial(handover_kernel, nz, nt), out_shape=tupl...]
    another operation x4 -> x0, other arithmetic: 5.41 us -> none  [the longest x2 3.74 us: kernel_plan(): jnp.stack([(norm_gain * jnp.swapaxes(expert_gate, 1, 2)).astype(jnp.bfloa...]
    convert_element_type x3 -> x0, other arithmetic: 4.79 us -> none  [the longest x1 2.14 us: kernel_plan(): normed = (widened * lax.rsqrt(jnp.mean(widened * widened, axis=1, keepdim...]
    reduce_sum x3 -> x0, other arithmetic: 3.39 us -> none  [the longest x1 1.38 us: kernel_plan(): jnp.mean(widened * widened, axis=1, keepdims=True) + EPSILON]
    slice x1 -> x0, local copies, waits for them, and re-layouts: 3.11 us -> none  [kernel_plan(): wall[2][None]]
    unnamed x16 -> x17, local copies, waits for them, and re-layouts: 5.79 us -> 8.39 us
where the time goes in v2:
time: 153 us
  Pallas kernels  144 us (94%)
  local copies, waits for them, and re-layouts  8.39 us (5%)
    pallas_call x1, Pallas kernels, kernel_plan(): pl.pallas_call(functools.partial(handover_kernel, nz, nt), out_shape=tupl...  144 us
    unnamed x17, local copies, waits for them, and re-layouts  8.39 us

profile of v2, /device:TPU:0, one launch (start us, length us, event | category | flops | bytes accessed | tf_op | source)
XLA Modules:
  0.0 153.1 jit_solution(16952069534493303496)
XLA Ops:
  0.6 144.1 %shard_map.153 = (bf16[128,2048]{1,0:T(8,128)(2,1)}, bf16[2048,256]{1,0:T(8,128)(2,1)}, bf16[2048,256]{1,0:T(8,128)(2,1)}, bf16[256,2048]{1,0:T(8,128)(2,1)}, bf...) custom-call(bf16[128,2048]{1,0:T(8,128)(2,1)} %tokens.1, s32[8,128]{1,0:T(8,128)} %bitcast.17, ...), custom_call_target="tpu_custom_call" | custom-call | tf_op jit(solution)/shard_map/pallas_call | solution.py:874
  144.7 0.0 copy-start.1
  144.7 2.0 %copy.24 = bf16[128,2048]{1,0:T(8,128)(2,1)} copy(bf16[128,2048]{1,0:T(8,128)(2,1)} %get-tuple-element.28) | data formatting | bytes 1048576
  146.7 0.0 copy-start
  146.7 2.4 %copy.25 = bf16[1,2048,256]{2,1,0:T(8,128)(2,1)} copy(bf16[1,2048,256]{2,1,0:T(8,128)(2,1)} %bitcast.14) | data formatting | bytes 2097152
  149.1 0.0 copy-done.1
  149.1 0.0 copy-start.4
  149.1 0.0 copy-start.3
  149.1 0.0 copy-start.2
  149.1 1.0 copy.26
  150.0 0.0 copy-done
  150.0 1.0 copy.27
  151.0 0.0 copy-done.4
  151.0 0.7 copy.28
  151.7 0.0 copy-done.3
  151.7 0.7 copy.29
  152.4 0.0 copy-done.2
  152.4 0.7 copy.30
Async XLA Ops:
  144.7 4.3 %copy-start.1 = (bf16[2048,256]{1,0:T(8,128)(2,1)S(1)}, bf16[2048,256]{1,0:T(8,128)(2,1)}, u32[]{:S(2)}) copy-start(bf16[2048,256]{1,0:T(8,128)(2,1)} %get-tuple-element.16) | copy-start | bytes 3145732
  146.7 3.3 %copy-start = (bf16[256,2048]{1,0:T(8,128)(2,1)S(1)}, bf16[256,2048]{1,0:T(8,128)(2,1)}, u32[]{:S(2)}) copy-start(bf16[256,2048]{1,0:T(8,128)(2,1)} %get-tuple-element.17) | copy-start | bytes 3145732
  149.1 2.0 %copy-start.4 = (bf16[512,256]{1,0:T(8,128)(2,1)S(1)}, bf16[512,256]{1,0:T(8,128)(2,1)}, u32[]{:S(2)}) copy-start(bf16[512,256]{1,0:T(8,128)(2,1)} %get-tuple-element.32) | copy-start | bytes 786436
  149.1 2.7 %copy-start.3 = (bf16[512,256]{1,0:T(8,128)(2,1)S(1)}, bf16[512,256]{1,0:T(8,128)(2,1)}, u32[]{:S(2)}) copy-start(bf16[512,256]{1,0:T(8,128)(2,1)} %get-tuple-element.33) | copy-start | bytes 786436
  149.1 3.4 %copy-start.2 = (bf16[64,2048]{1,0:T(8,128)(2,1)S(1)}, bf16[64,2048]{1,0:T(8,128)(2,1)}, u32[]{:S(2)}) copy-start(bf16[64,2048]{1,0:T(8,128)(2,1)} %get-tuple-element.34) | copy-start | bytes 786436

commit v3 on v2

--- a/solution.py
+++ b/solution.py
@@ -9,6 +9,7 @@
 EPSILON = 1e-06
 route_scale = 2.5
 CORES = 2
+PIECES = 2
 MESH = pl.DeviceIdType.MESH
 
 
@@ -118,6 +119,17 @@
     return (mixed, served_gate, served_up, served_down, held_gate, held_up, held_down)
 
 
+def plane_orders(nz):
+    far = [p for p in [nz - 2, nz - 1] + list(range(nz - 3, 0, -1)) if p > 0]
+    orders = []
+    for z in range(nz):
+        low = 2 * z < nz
+        q = z if low else nz - 1 - z
+        planes = [p for p in [0] + far if p != q] + [q]
+        orders.append(planes if low else [nz - 1 - p for p in planes])
+    return orders
+
+
 def handover_kernel(
     nz,
     nt,
@@ -178,7 +190,9 @@
     srecv,
     hsend,
     hrecv,
-    asend,
+    azsend,
+    axsend,
+    acsend,
     arecv,
     rdsend,
     rdrecv,
@@ -323,14 +337,14 @@
             rem(
                 gu.at[j, pl.ds(0, 2), pl.ds(al(gg * half_f, half_f), half_f), :],
                 gu_at(me, gg),
-                ssem.at[0, j],
+                ssem.at[0],
                 rsem.at[0, me],
                 device,
             ),
             rem(
                 dn.at[j, pl.ds(al(gg * half_r, half_r), half_r), :],
                 dn_at(me, gg),
-                ssem.at[1, j],
+                ssem.at[1],
                 rsem.at[1, me],
                 device,
             ),
@@ -340,28 +354,30 @@
         return w_send(j, g, wsend, wrecv)
 
     def w_mate():
-        return w_send(mate, 1 - g, ysend, yrecv)
+        return w_send(mate, 1 - g, wsend, yrecv)
 
     def w_across(s, gg):
         return (
-            rem(gu_at(s, gg), gu_at(s, gg), ysend.at[0, s], yrecv.at[0, s], across),
-            rem(dn_at(s, gg), dn_at(s, gg), ysend.at[1, s], yrecv.at[1, s], across),
+            rem(gu_at(s, gg), gu_at(s, gg), ysend.at[0], yrecv.at[0, s], across),
+            rem(dn_at(s, gg), dn_at(s, gg), ysend.at[1], yrecv.at[1, s], across),
         )
 
     def w_plane_send(p):
         @pl.loop(0, nt)
-        def _(tt):
-            for cp in w_out(p * nt + tt):
+        def _(k):
+            for cp in w_out(p * nt + lax.rem(t + k, nt)):
                 cp.start()
 
-    def w_plane_across(p):
+    def w_planes_across(count, plane):
         @pl.loop(0, nt)
-        def _(tt):
-            s = p * nt + tt
-            for i, at in ((0, gu_at), (1, dn_at)):
-                rem(at(s, g), at(s, g), ysend.at[i, s], wrecv.at[i, s], across).wait_recv()
-            for cp in w_across(s, g):
-                cp.start()
+        def _(k):
+            @pl.loop(0, count)
+            def _(i):
+                s = plane(i) * nt + lax.rem(t + nt - k, nt)
+                for m, at in ((0, gu_at), (1, dn_at)):
+                    rem(at(s, g), at(s, g), ysend.at[0], wrecv.at[m, s], across).wait_recv()
+                for cp in w_across(s, g):
+                    cp.start()
 
     def share_send(j):
         return rem(shares.at[j], share.at[me], shsend.at[j], shrecv.at[me], dev(j // nt, j % nt))
@@ -409,35 +425,35 @@
             rem(
                 sgu.at[pl.ds(0, 2), pl.ds(al(g * half_st, half_st), half_st), :],
                 hgu_half(t, g),
-                hsend.at[0, t],
-                hrecv.at[0, t],
+                hsend.at[0, x],
+                hrecv.at[0, x],
                 xdev(k),
             ),
             rem(
                 sdn.at[pl.ds(al(g * half_sr, half_sr), half_sr), :],
                 hd_half(t, g),
-                hsend.at[1, t],
-                hrecv.at[1, t],
+                hsend.at[1, x],
+                hrecv.at[1, x],
                 xdev(k),
             ),
         )
 
     def held_x_in(ts):
         return (
-            rem(hgu_half(ts, g), hgu_half(ts, g), hsend.at[0, ts], hrecv.at[0, ts], across),
-            rem(hd_half(ts, g), hd_half(ts, g), hsend.at[1, ts], hrecv.at[1, ts], across),
+            rem(hgu_half(ts, g), hgu_half(ts, g), hsend.at[0, ts // CORES], hrecv.at[0, ts // CORES], across),
+            rem(hd_half(ts, g), hd_half(ts, g), hsend.at[1, ts // CORES], hrecv.at[1, ts // CORES], across),
         )
 
     def held_across(ts, gg):
         return (
-            rem(hgu_half(ts, gg), hgu_half(ts, gg), hsend.at[2, ts], hrecv.at[2, ts], across),
-            rem(hd_half(ts, gg), hd_half(ts, gg), hsend.at[3, ts], hrecv.at[3, ts], across),
+            rem(hgu_half(ts, gg), hgu_half(ts, gg), hsend.at[2, ts // CORES], hrecv.at[2, ts // CORES], across),
+            rem(hd_half(ts, gg), hd_half(ts, gg), hsend.at[3, ts // CORES], hrecv.at[3, ts // CORES], across),
         )
 
     def held_core(ts):
         return (
-            rem(hgu_at(ts), hgu_at(ts), hsend.at[4, ts], hrecv.at[4, ts], partner),
-            rem(hd_at(ts), hd_at(ts), hsend.at[5, ts], hrecv.at[5, ts], partner),
+            rem(hgu_at(ts), hgu_at(ts), hsend.at[4, ts // CORES], hrecv.at[4, ts // CORES], partner),
+            rem(hd_at(ts), hd_at(ts), hsend.at[5, ts // CORES], hrecv.at[5, ts // CORES], partner),
         )
 
     def a_z(p, up):
@@ -445,21 +461,21 @@
         return rem(
             tok.at[s],
             tok.at[s],
-            asend.at[0 if up else 1, s],
+            azsend.at[0 if up else 1, p],
             arecv.at[s],
             dev(z + 1 if up else z - 1, t),
         )
 
     def a_x(p, k):
         s = slot(p, c, x)
-        return rem(tok.at[s], tok.at[s], asend.at[2 + k, s], arecv.at[s], xdev(k))
+        return rem(tok.at[s], tok.at[s], axsend.at[p], arecv.at[s], xdev(k))
 
     def a_core(p, xb):
         s = slot(p, c, xb)
-        return rem(tok.at[s], tok.at[s], asend.at[2, s], arecv.at[s], partner)
+        return rem(tok.at[s], tok.at[s], acsend.at[p], arecv.at[s], partner)
 
     def a_wait(s):
-        rem(tok.at[s], tok.at[s], asend.at[2, s], arecv.at[s], partner).wait_recv()
+        rem(tok.at[s], tok.at[s], acsend.at[0], arecv.at[s], partner).wait_recv()
 
     def a_cross(p):
         for k in range(1, xc):
@@ -467,32 +483,49 @@
             a_wait(slot(p, c, xb))
             a_core(p, xb).start()
 
-    def r_core(p):
+    def r_core(p, xb):
         return rem(
-            part.at[pl.ds(slot(p, 1 - c, 0), xc)],
-            rd.at[pl.ds(p * xc, xc)],
+            part.at[slot(p, 1 - c, xb)],
+            rd.at[p * xc + xb],
             rdsend.at[p],
-            rdrecv.at[p],
+            rdrecv.at[p, xb],
             partner,
         )
 
-    def r_x(p, k):
+    piece = rows // PIECES
+
+    def band_of(f):
+        return pl.ds(al(f * piece, piece), piece)
+
+    def r_x(p, k, f):
         xb = lax.rem(x + k, xc)
         return rem(
-            part.at[slot(p, c, xb)],
-            rx.at[p * (xc - 1) + k - 1],
-            rxsend.at[p, k - 1],
-            rxrecv.at[p, k - 1],
+            part.at[slot(p, c, xb), band_of(f)],
+            rx.at[p * (xc - 1) + k - 1, band_of(f)],
+            rxsend.at[p],
+            rxrecv.at[p * (xc - 1) + k - 1, f],
             xdev(k),
         )
 
-    def r_z(p):
-        return rem(part.at[slot(p, c, x)], rz.at[z], rzsend.at[p], rzrecv.at[z], dev(p, t))
+    def r_z(p, f):
+        return rem(
+            part.at[slot(p, c, x), band_of(f)],
+            rz.at[z, band_of(f)],
+            rzsend.at[p],
+            rzrecv.at[z, f],
+            dev(p, t),
+        )
 
     near = jnp.where(z == 0, 1, nz - 2)
 
-    def r_relay(p):
-        return rem(part.at[slot(p, c, x)], ry.at[p], rzsend.at[p], ryrecv.at[p], dev(near, t))
+    def r_relay(p, f):
+        return rem(
+            part.at[slot(p, c, x), band_of(f)],
+            ry.at[p, band_of(f)],
+            rzsend.at[p],
+            ryrecv.at[p, f],
+            dev(near, t),
+        )
 
     def relayed(p):
         return ((z == 1) & (p > 1)) | ((z == nz - 2) & (p < nz - 2))
@@ -526,12 +559,18 @@
         def _():
             cp.start()
 
-    last = jnp.where(2 * z < nz, nz - 1 - z, z)
 
     edge = (z == 0) | (z == nz - 1)
+    low = 2 * z < nz
 
     @pl.loop(0, nz + 1)
     def _(d):
+        @pl.when(~edge & (d == 2))
+        def _():
+            w_planes_across(
+                jnp.where(low, z, nz - 1 - z), lambda i: jnp.where(low, z - 1 - i, z + 1 + i)
+            )
+
         late = edge & (d == nz - 1)
 
         @pl.when((d > 0) & (z - d >= 0) & ~late)
@@ -570,19 +609,17 @@
                 for cp in held_x(k):
                     cp.start()
 
-        @pl.when(d < nz)
-        def _():
-            stop = jnp.where(edge | (d < last), d, nz - 1)
-
-            @pl.loop(d, stop + 1)
-            def _(q):
-                @pl.when((q > z) & (edge | (d <= last)))
+        @pl.when((edge & (d == 0)) | (~edge & (d == 1)))
+        def _():
+            @pl.loop(1, nz)
+            def _(k):
+                @pl.when(z + k < nz)
                 def _():
-                    w_plane_send(q)
-
-                @pl.when((nz - 1 - q < z) & (edge | (d <= last)))
+                    w_plane_send(z + k)
+
+                @pl.when(z - k >= 0)
                 def _():
-                    w_plane_send(nz - 1 - q)
+                    w_plane_send(z - k)
 
         @pl.when(d == 1)
         def _():
@@ -590,7 +627,7 @@
             def _(k):
                 s = z * nt + lax.rem(t + k, nt)
                 for i, at in ((0, gu_at), (1, dn_at)):
-                    rem(at(s, g), at(s, g), ysend.at[i, s], wrecv.at[i, s], across).wait_recv()
+                    rem(at(s, g), at(s, g), ysend.at[0], wrecv.at[i, s], across).wait_recv()
 
                 @pl.when(s != mate)
                 def _():
@@ -599,34 +636,33 @@
 
         @pl.when(late)
         def _():
+            w_planes_across(1, lambda i: near)
+            w_planes_across(1, lambda i: nz - 1 - z)
             p = nz - 1 - z
-            w_plane_across(p)
             a_wait(slot(p, c, x))
             for k in range(1, xc):
                 a_x(p, k).start()
             a_core(p, x).start()
 
-        @pl.when((d == z + 1) & (z < nz - 1))
-        def _():
-            @pl.loop(0, z)
-            def _(p):
-                w_plane_across(p)
-
-        @pl.when((d == nz - z) & (z > 0))
-        def _():
-            @pl.loop(z + 1, nz)
-            def _(k):
-                w_plane_across(nz + z - k)
+        @pl.when(~edge & (d == nz))
+        def _():
+            w_planes_across(
+                jnp.where(low, nz - 1 - z, z), lambda i: jnp.where(low, z + 1 + i, z - 1 - i)
+            )
 
         @pl.when(edge & (d == nz))
         def _():
-            @pl.loop(1, nz - 1)
-            def _(k):
-                w_plane_across(jnp.where(z == 0, nz - 1 - k, k))
+            w_planes_across(nz - 3, lambda i: jnp.where(z == 0, nz - 2 - i, 1 + i))
+
+    tail = jnp.where(low, nz - 1, 0)
 
     @pl.loop(0, nz)
     def _(k):
-        a_cross(lax.rem(z + k, nz))
+        p = lax.rem(z + k, nz)
+
+        @pl.when(p != tail)
+        def _():
+            a_cross(p)
 
     for k in range(1, xc):
         ts = lax.rem(x + k, xc) * CORES + c
@@ -658,69 +694,77 @@
     out_down.start()
     nt_dims = (((1,), (1,)), ((), ()))
 
-    def compute(p, h):
-        first = slot(p, h, 0)
-        xs = tok[pl.ds(first, xc)].reshape(xc * rows, width)
+    def compute(p, h, xb):
+        at = slot(p, h, xb)
+        xs = tok[at]
         gate = lax.dot_general(xs, w[0], nt_dims, preferred_element_type=jnp.float32)
         up = lax.dot_general(xs, w[1], nt_dims, preferred_element_type=jnp.float32)
         hidden = gate / (1.0 + jnp.exp(-gate)) * up
-        scale = jnp.concatenate(
-            [
-                jnp.transpose(jnp.broadcast_to(share[p * nt + xb * CORES + h], (rows, rows)))
-                for xb in range(xc)
-            ],
-            axis=0,
+        scale = jnp.transpose(
+            jnp.broadcast_to(share[p * nt + xb * CORES + h], (rows, rows))
         )[:, :1]
         col = lax.broadcasted_iota(jnp.int32, hidden.shape, 1)
         hidden = jnp.where(col < inner, hidden * scale, hidden).astype(jnp.bfloat16)
         step = min(512, width)
         for lo in range(0, width, step):
             res = jnp.dot(hidden, w[2, :, lo : lo + step], preferred_element_type=jnp.float32)
-            part[pl.ds(first, xc), :, lo : lo + step] = res.astype(jnp.bfloat16).reshape(
-                xc, rows, step
-            )
+            part[at, :, lo : lo + step] = res.astype(jnp.bfloat16)
 
     def work(p):
+        @pl.when(p == tail)
+        def _():
+            a_cross(p)
+
         for xb in range(xc):
             a_wait(slot(p, 1 - c, xb))
 
-        @pl.loop(0, 2)
+        @pl.loop(0, 2 * xc)
         def _(j):
-            compute(p, (1 - c) * (1 - j) + c * j)
-
-            @pl.when(j == 0)
+            k = lax.rem(j // 2 + 1, xc)
+            xb = lax.rem(x + k, xc)
+            mine = lax.rem(j, 2)
+            compute(p, (1 - c) * (1 - mine) + c * mine, xb)
+
+            @pl.when(mine == 0)
             def _():
-                r_core(p).start()
-
-        r_core(p).wait_recv()
+                r_core(p, xb).start()
+
+            for k2 in range(1, xc):
+                @pl.when((mine == 1) & (k == k2))
+                def _():
+                    r_core(p, xb).wait_recv()
+                    s = slot(p, c, xb)
+                    part[s] = (
+                        part[s].astype(jnp.float32) + rd[p * xc + xb].astype(jnp.float32)
+                    ).astype(jnp.bfloat16)
+                    for f in range(PIECES):
+                        r_x(p, k2, f).start()
+
+    def settle(p, f):
+        s = slot(p, c, x)
+        at = band_of(f)
+
+        @pl.when(f == 0)
+        def _():
+            r_core(p, x).wait_recv()
+
+        acc = part[s, at].astype(jnp.float32) + rd[p * xc + x, at].astype(jnp.float32)
         for k in range(1, xc):
-            xb = lax.rem(x + k, xc)
-            s = slot(p, c, xb)
-            part[s] = (part[s].astype(jnp.float32) + rd[p * xc + xb].astype(jnp.float32)).astype(
-                jnp.bfloat16
-            )
-            r_x(p, k).start()
-
-    def settle(p):
-        s = slot(p, c, x)
-        acc = part[s].astype(jnp.float32) + rd[p * xc + x].astype(jnp.float32)
-        for k in range(1, xc):
-            r_x(p, k).wait_recv()
-            acc = acc + rx[p * (xc - 1) + k - 1].astype(jnp.float32)
-        part[s] = acc.astype(jnp.bfloat16)
+            r_x(p, k, f).wait_recv()
+            acc = acc + rx[p * (xc - 1) + k - 1, at].astype(jnp.float32)
+        part[s, at] = acc.astype(jnp.bfloat16)
 
         @pl.when(relayed(p))
         def _():
-            r_relay(p).wait_recv()
-            part[s] = (acc + ry[p].astype(jnp.float32)).astype(jnp.bfloat16)
-
-    low = 2 * z < nz
+            r_relay(p, f).wait_recv()
+            part[s, at] = (acc + ry[p, at].astype(jnp.float32)).astype(jnp.bfloat16)
 
     def order(i):
-        q = jnp.where(edge, i, jnp.where(i == 0, 0, nz - i))
-        inside = jnp.where(q == 0, jnp.where(low, 0, nz - 1), jnp.where(low, q, nz - 1 - q))
-        ends = jnp.where(low, nz - 1 - i, i)
-        return jnp.where(i == nz - 1, z, jnp.where(edge, ends, inside))
+        q = jnp.int32(0)
+        for zz, planes in enumerate(plane_orders(nz)):
+            for ii, p in enumerate(planes):
+                q = jnp.where((z == zz) & (i == ii), p, q)
+        return q
 
     @pl.loop(0, nz)
     def _(i):
@@ -737,15 +781,18 @@
         @pl.when(i > 0)
         def _():
             p = order(i - 1)
-            settle(p)
-
-            @pl.when(edge & (p != near))
-            def _():
-                r_relay(p).start()
-
-            @pl.when(~edge | (p == near))
-            def _():
-                r_z(p).start()
+
+            @pl.loop(0, PIECES)
+            def _(f):
+                settle(p, f)
+
+                @pl.when(edge & (p != near))
+                def _():
+                    r_relay(p, f).start()
+
+                @pl.when(~edge | (p == near))
+                def _():
+                    r_z(p, f).start()
 
     for k in range(1, xc):
         ts = lax.rem(x + k, xc) * CORES + c
@@ -762,33 +809,38 @@
     out_held = [
         pltpu.make_async_copy(hflip.at[0], o_hgate, osem.at[3]),
         pltpu.make_async_copy(hflip.at[1], o_hup, osem.at[4]),
-        pltpu.make_async_copy(hd, o_hd, osem.at[6]),
+        pltpu.make_async_copy(hd, o_hd, osem.at[5 + PIECES]),
     ]
     for cp in out_held:
         cp.start()
 
-    settle(z)
-    total[...] = part[own].astype(jnp.float32)
-    for k in range(1, nz):
-        zs = lax.rem(z + k, nz)
-
-        @pl.when(((zs > 0) & (zs < nz - 1)) | (zs == z + 1) | (zs == z - 1))
-        def _():
-            rem(rz.at[zs], rz.at[zs], rzsend.at[zs], rzrecv.at[zs], partner).wait_recv()
-            total[...] += rz[zs].astype(jnp.float32)
-
-    l_tok[...] = total[...].astype(jnp.bfloat16)
-    out_mix = pltpu.make_async_copy(l_tok, o_mix, osem.at[5])
-    out_mix.start()
-
+    @pl.loop(0, PIECES)
+    def _(f):
+        at = band_of(f)
+        settle(z, f)
+        total[at] = part[own, at].astype(jnp.float32)
+        for k in range(1, nz):
+            zs = lax.rem(z + k, nz)
+
+            @pl.when(((zs > 0) & (zs < nz - 1)) | (zs == z + 1) | (zs == z - 1))
+            def _():
+                rem(rz.at[zs, at], rz.at[zs, at], rzsend.at[0], rzrecv.at[zs, f], partner).wait_recv()
+                total[at] += rz[zs, at].astype(jnp.float32)
+
+        l_tok[at] = total[at].astype(jnp.bfloat16)
+        pltpu.make_async_copy(l_tok.at[at], o_mix.at[at], osem.at[5 + f]).start()
+
+    def sent(ref, sem):
+        rem(ref, ref, sem, acsend.at[0], partner).wait_send()
+
+    sent(gu.at[:, :, pl.ds(0, half_f), :], wsend.at[0])
+    sent(dn.at[:, pl.ds(0, half_r), :], wsend.at[1])
+    sent(gu.at[pl.ds(0, n - 2), :, pl.ds(0, half_f), :], ysend.at[0])
+    sent(dn.at[pl.ds(0, n - 2), pl.ds(0, half_r), :], ysend.at[1])
     @pl.loop(1, n)
     def _(k):
-        j = lax.rem(me + k, n)
-        for cp in w_out(j):
-            cp.wait_send()
-        share_send(j).wait_send()
-        for cp in w_across(j, g):
-            cp.wait_send()
+        share_send(lax.rem(me + k, n)).wait_send()
+
 
     for send, count in ((sgu_send, nz), (sdn_send, nt)):
         for k in range(count):
@@ -817,23 +869,48 @@
         def _():
             a_z(p, False).wait_send()
 
-        for k in range(1, xc):
-            a_x(p, k).wait_send()
-            r_x(p, k).wait_send()
-        for xb in range(xc):
-            a_core(p, xb).wait_send()
-        r_core(p).wait_send()
+        sent(tok.at[pl.ds(0, xc - 1)], axsend.at[p])
+        sent(tok.at[pl.ds(0, xc)], acsend.at[p])
+        sent(part.at[pl.ds(0, xc)], rdsend.at[p])
+        sent(part.at[pl.ds(0, xc - 1)], rxsend.at[p])
 
         @pl.when(p != z)
         def _():
-            r_z(p).wait_send()
+            sent(part.at[0], rzsend.at[p])
 
     out_down.wait()
     for i, o_w in enumerate((o_gate, o_up)):
         pltpu.make_async_copy(flip.at[i], o_w, osem.at[1 + i]).wait()
     for cp in out_held:
         cp.wait()
-    out_mix.wait()
+    for f in range(PIECES):
+        pltpu.make_async_copy(l_tok.at[band_of(f)], o_mix.at[band_of(f)], osem.at[5 + f]).wait()
+
+
+def deliver_kernel(*refs):
+    count = (len(refs) - 1) // 3
+    src, dst, buf = refs[:count], refs[count : 2 * count], refs[2 * count : 3 * count]
+    sems = refs[3 * count]
+    for i in range(count):
+        pltpu.make_async_copy(src[i], buf[i], sems.at[0, i]).start()
+    for i in range(count):
+        pltpu.make_async_copy(src[i], buf[i], sems.at[0, i]).wait()
+        pltpu.make_async_copy(buf[i], dst[i], sems.at[1, i]).start()
+    for i in range(count):
+        pltpu.make_async_copy(buf[i], dst[i], sems.at[1, i]).wait()
+
+
+def deliver(arrays):
+    hbm = pl.BlockSpec(memory_space=pltpu.HBM)
+    count = len(arrays)
+    return pl.pallas_call(
+        deliver_kernel,
+        out_shape=tuple(jax.ShapeDtypeStruct(a.shape, a.dtype) for a in arrays),
+        in_specs=[hbm] * count,
+        out_specs=(hbm,) * count,
+        scratch_shapes=[pltpu.VMEM(a.shape, a.dtype) for a in arrays]
+        + [pltpu.SemaphoreType.DMA((2, count))],
+    )(*arrays)
 
 
 def kernel_plan(
@@ -871,7 +948,7 @@
         (dt, st * nt),
         (sr, width),
     )
-    mixed, gate, up, down, hgate, hup, hd = pl.pallas_call(
+    made = pl.pallas_call(
         functools.partial(handover_kernel, nz, nt),
         out_shape=tuple(jax.ShapeDtypeStruct(s, bf) for s in outs),
         in_specs=[hbm] * 10,
@@ -906,26 +983,28 @@
             pltpu.VMEM((2, width, inner), bf),
             pltpu.VMEM((2, dt, st * nt), bf),
             dma((10,)),
-            dma((7,)),
+            dma((6 + PIECES,)),
+            dma((2,)),
             dma((2, n)),
-            dma((2, n)),
-            dma((2, n)),
+            dma((2,)),
             dma((2, n)),
             dma((n,)),
             dma((n,)),
             dma((2, max(nz, nt))),
             dma((2, max(nz, nt))),
-            dma((6, nt)),
-            dma((6, nt)),
-            dma((2 + xc, n)),
+            dma((6, xc)),
+            dma((6, xc)),
+            dma((2, nz)),
+            dma((nz,)),
+            dma((nz,)),
             dma((n,)),
             dma((nz,)),
-            dma((nz,)),
-            dma((nz, xc)),
             dma((nz, xc)),
             dma((nz,)),
+            dma((nz * (xc - 1), PIECES)),
             dma((nz,)),
-            dma((nz,)),
+            dma((nz, PIECES)),
+            dma((nz, PIECES)),
         ],
         compiler_params=pltpu.CompilerParams(
             collective_id=0, has_side_effects=True, vmem_limit_bytes=60 << 20
@@ -942,6 +1021,7 @@
         shared_up.T,
         shared_down,
     )
+    mixed, gate, up, down, hgate, hup, hd = deliver(made)
     return mixed, gate[None], up[None], down[None], hgate, hup, hd
 
 

time: 153 us -> 136 us (0.89)
  local copies, waits for them, and re-layouts: 8.39 us -> 0 us
  Pallas kernels: 144 us -> 136 us
    pallas_call x1, Pallas kernels: 144 us -> 132 us  [kernel_plan(): pl.pallas_call(functools.partial(handover_kernel, nz, nt), out_shape=tupl...]
    unnamed x17 -> x0, local copies, waits for them, and re-layouts: 8.39 us -> none
    pallas_call x0 -> x1, Pallas kernels: none -> 3.54 us  [deliver(): pl.pallas_call(deliver_kernel, out_shape=tuple((jax.ShapeDtypeStruct(a.sh...]
where the time goes in v3:
time: 136 us
  Pallas kernels  136 us (100%)
    pallas_call x1, Pallas kernels, kernel_plan(): pl.pallas_call(functools.partial(handover_kernel, nz, nt), out_shape=tupl...  132 us
    pallas_call x1, Pallas kernels, deliver(): pl.pallas_call(deliver_kernel, out_shape=tuple((jax.ShapeDtypeStruct(a.sh...  3.54 us

profile of v3, /device:TPU:0, one launch (start us, length us, event | category | flops | bytes accessed | tf_op | source)
XLA Modules:
  0.0 136.3 jit_solution(16687074988464702134)
XLA Ops:
  0.6 132.1 %shard_map.153 = (bf16[128,2048]{1,0:T(8,128)(2,1)}, bf16[2048,256]{1,0:T(8,128)(2,1)}, bf16[2048,256]{1,0:T(8,128)(2,1)}, bf16[256,2048]{1,0:T(8,128)(2,1)}, bf...) custom-call(bf16[128,2048]{1,0:T(8,128)(2,1)} %tokens.1, s32[8,128]{1,0:T(8,128)} %bitcast.14, ...), custom_call_target="tpu_custom_call" | custom-call | tf_op jit(solution)/shard_map/pallas_call | solution.py:951
  132.7 3.5 %shard_map.154 = (bf16[128,2048]{1,0:T(8,128)(2,1)}, bf16[2048,256]{1,0:T(8,128)(2,1)}, bf16[2048,256]{1,0:T(8,128)(2,1)}, bf16[256,2048]{1,0:T(8,128)(2,1)}, bf...) custom-call(bf16[128,2048]{1,0:T(8,128)(2,1)} %get-tuple-element.21.refs_0_, ...), custom_call_target="tpu_custom_call" | custom-call | tf_op jit(solution)/shard_map/pallas_call | solution.py:906

commit v4 on v3

--- a/solution.py
+++ b/solution.py
@@ -9,7 +9,7 @@
 EPSILON = 1e-06
 route_scale = 2.5
 CORES = 2
-PIECES = 2
+PIECES = 4
 MESH = pl.DeviceIdType.MESH
 
 
@@ -120,12 +120,13 @@
 
 
 def plane_orders(nz):
-    far = [p for p in [nz - 2, nz - 1] + list(range(nz - 3, 0, -1)) if p > 0]
     orders = []
     for z in range(nz):
         low = 2 * z < nz
         q = z if low else nz - 1 - z
-        planes = [p for p in [0] + far if p != q] + [q]
+        first = [1] if q == 0 else [0]
+        far = [p for p in range(nz - 1, 0, -1) if p != q and p not in first]
+        planes = first + (far + [q] if q == 0 else [q] + far)
         orders.append(planes if low else [nz - 1 - p for p in planes])
     return orders
 
@@ -172,6 +173,7 @@
     rx,
     rz,
     ry,
+    rp,
     total,
     share,
     hgu,
@@ -201,6 +203,8 @@
     rzsend,
     rzrecv,
     ryrecv,
+    rpsend,
+    rprecv,
 ):
     n = nz * nt
     xc = nt // CORES
@@ -331,35 +335,35 @@
         zs, ts = src // nt, src % nt
         return w.at[2, pl.ds(al(zs * fr + gg * half_r, half_r), half_r), pl.ds(al(ts * dc, dc), dc)]
 
-    def w_send(j, gg, ssem, rsem):
+    def w_send(j, gg, rsems):
         device = dev(j // nt, j % nt)
         return (
             rem(
                 gu.at[j, pl.ds(0, 2), pl.ds(al(gg * half_f, half_f), half_f), :],
                 gu_at(me, gg),
-                ssem.at[0],
-                rsem.at[0, me],
+                wsend.at[0],
+                rsems[0],
                 device,
             ),
             rem(
                 dn.at[j, pl.ds(al(gg * half_r, half_r), half_r), :],
                 dn_at(me, gg),
-                ssem.at[1],
-                rsem.at[1, me],
+                wsend.at[1],
+                rsems[1],
                 device,
             ),
         )
 
     def w_out(j):
-        return w_send(j, g, wsend, wrecv)
+        return w_send(j, g, (wrecv.at[0, me], wrecv.at[1, me]))
 
     def w_mate():
-        return w_send(mate, 1 - g, wsend, yrecv)
+        return w_send(mate, 1 - g, (yrecv.at[0], yrecv.at[1]))
 
     def w_across(s, gg):
         return (
-            rem(gu_at(s, gg), gu_at(s, gg), ysend.at[0], yrecv.at[0, s], across),
-            rem(dn_at(s, gg), dn_at(s, gg), ysend.at[1], yrecv.at[1, s], across),
+            rem(gu_at(s, gg), gu_at(s, gg), ysend.at[0], yrecv.at[0], across),
+            rem(dn_at(s, gg), dn_at(s, gg), ysend.at[1], yrecv.at[1], across),
         )
 
     def w_plane_send(p):
@@ -527,6 +531,23 @@
             dev(near, t),
         )
 
+    first = PIECES // 2 if nz != 3 else 0
+    pair = jnp.where(
+        (z == 0) | (z == nz - 1), near, jnp.where(z == 1, 0, jnp.where(z == nz - 2, nz - 1, -1))
+    )
+    if first == 0:
+        pair = jnp.int32(-1)
+
+    def r_pair(k, f):
+        xb = lax.rem(x + k, xc)
+        return rem(
+            part.at[slot(pair, c, xb), band_of(f)],
+            rp.at[k - 1, band_of(f)],
+            rpsend,
+            rprecv.at[k - 1, f],
+            dev(pair, t),
+        )
+
     def relayed(p):
         return ((z == 1) & (p > 1)) | ((z == nz - 2) & (p < nz - 2))
 
@@ -638,6 +659,7 @@
         def _():
             w_planes_across(1, lambda i: near)
             w_planes_across(1, lambda i: nz - 1 - z)
+            w_planes_across(nz - 3, lambda i: jnp.where(z == 0, nz - 2 - i, 1 + i))
             p = nz - 1 - z
             a_wait(slot(p, c, x))
             for k in range(1, xc):
@@ -649,10 +671,6 @@
             w_planes_across(
                 jnp.where(low, nz - 1 - z, z), lambda i: jnp.where(low, z + 1 + i, z - 1 - i)
             )
-
-        @pl.when(edge & (d == nz))
-        def _():
-            w_planes_across(nz - 3, lambda i: jnp.where(z == 0, nz - 2 - i, 1 + i))
 
     tail = jnp.where(low, nz - 1, 0)
 
@@ -671,11 +689,14 @@
         for cp in held_across(ts, g):
             cp.start()
 
+    others = gu.at[pl.ds(0, n - 1), :, pl.ds(0, half_f), :]
+    rem(others, others, ysend.at[0], yrecv.at[0], across).wait_recv()
+    others = dn.at[pl.ds(0, n - 1), pl.ds(0, half_r), :]
+    rem(others, others, ysend.at[1], yrecv.at[1], across).wait_recv()
+
     @pl.loop(1, n)
     def _(k):
         s = lax.rem(me + n - k, n)
-        for cp in w_across(s, 1 - g):
-            cp.wait_recv()
         rem(shares.at[s], share.at[s], shsend.at[s], shrecv.at[s], across).wait_recv()
 
     for k in range(nz):
@@ -737,27 +758,49 @@
                     part[s] = (
                         part[s].astype(jnp.float32) + rd[p * xc + xb].astype(jnp.float32)
                     ).astype(jnp.bfloat16)
-                    for f in range(PIECES):
+                    for f in range(first, PIECES):
                         r_x(p, k2, f).start()
-
-    def settle(p, f):
+                    for f in range(first):
+                        @pl.when(p == pair)
+                        def _():
+                            r_pair(k2, f).start()
+
+                        @pl.when((p == z) & (pair >= 0))
+                        def _():
+                            r_pair(k2, f).wait_recv()
+                            at = band_of(f)
+                            part[s, at] = (
+                                part[s, at].astype(jnp.float32)
+                                + rp[k2 - 1, at].astype(jnp.float32)
+                            ).astype(jnp.bfloat16)
+
+                        @pl.when(p != pair)
+                        def _():
+                            r_x(p, k2, f).start()
+
+    def settle(p, turn):
         s = slot(p, c, x)
+        f = jnp.where(p == pair, turn, lax.rem(turn + first, PIECES))
         at = band_of(f)
 
-        @pl.when(f == 0)
+        @pl.when(turn == 0)
         def _():
             r_core(p, x).wait_recv()
 
-        acc = part[s, at].astype(jnp.float32) + rd[p * xc + x, at].astype(jnp.float32)
-        for k in range(1, xc):
-            r_x(p, k, f).wait_recv()
-            acc = acc + rx[p * (xc - 1) + k - 1, at].astype(jnp.float32)
-        part[s, at] = acc.astype(jnp.bfloat16)
+        total[at] = part[s, at].astype(jnp.float32) + rd[p * xc + x, at].astype(jnp.float32)
+
+        @pl.when((p != pair) | (f >= first))
+        def _():
+            for k in range(1, xc):
+                r_x(p, k, f).wait_recv()
+                total[at] += rx[p * (xc - 1) + k - 1, at].astype(jnp.float32)
 
         @pl.when(relayed(p))
         def _():
             r_relay(p, f).wait_recv()
-            part[s, at] = (acc + ry[p, at].astype(jnp.float32)).astype(jnp.bfloat16)
+            total[at] += ry[p, at].astype(jnp.float32)
+
+        return f, at
 
     def order(i):
         q = jnp.int32(0)
@@ -766,9 +809,34 @@
                 q = jnp.where((z == zz) & (i == ii), p, q)
         return q
 
+    def emit(p, turn):
+        f, at = settle(p, turn)
+        part[slot(p, c, x), at] = total[at].astype(jnp.bfloat16)
+
+        @pl.when(edge & (p != near))
+        def _():
+            r_relay(p, f).start()
+
+        @pl.when(~edge | (p == near))
+        def _():
+            r_z(p, f).start()
+
+    def emit_rest(p):
+        @pl.when(p != z)
+        def _():
+            @pl.loop(jnp.where(p == pair, first, 0), PIECES)
+            def _(turn):
+                emit(p, turn)
+
     @pl.loop(0, nz)
     def _(i):
         work(order(i))
+
+        @pl.when((i == 0) & (pair >= 0))
+        def _():
+            @pl.loop(0, first)
+            def _(turn):
+                emit(pair, turn)
 
         @pl.when(i == 0)
         def _():
@@ -780,19 +848,9 @@
 
         @pl.when(i > 0)
         def _():
-            p = order(i - 1)
-
-            @pl.loop(0, PIECES)
-            def _(f):
-                settle(p, f)
-
-                @pl.when(edge & (p != near))
-                def _():
-                    r_relay(p, f).start()
-
-                @pl.when(~edge | (p == near))
-                def _():
-                    r_z(p, f).start()
+            emit_rest(order(i - 1))
+
+    emit_rest(order(nz - 1))
 
     for k in range(1, xc):
         ts = lax.rem(x + k, xc) * CORES + c
@@ -815,10 +873,8 @@
         cp.start()
 
     @pl.loop(0, PIECES)
-    def _(f):
-        at = band_of(f)
-        settle(z, f)
-        total[at] = part[own, at].astype(jnp.float32)
+    def _(turn):
+        f, at = settle(z, turn)
         for k in range(1, nz):
             zs = lax.rem(z + k, nz)
 
@@ -872,7 +928,17 @@
         sent(tok.at[pl.ds(0, xc - 1)], axsend.at[p])
         sent(tok.at[pl.ds(0, xc)], acsend.at[p])
         sent(part.at[pl.ds(0, xc)], rdsend.at[p])
-        sent(part.at[pl.ds(0, xc - 1)], rxsend.at[p])
+
+        @pl.when(p != pair)
+        def _():
+            sent(part.at[pl.ds(0, xc - 1)], rxsend.at[p])
+
+        if first > 0:
+            @pl.when(p == pair)
+            def _():
+                sent(part.at[pl.ds(0, xc - 1), pl.ds(0, rows - first * piece)], rxsend.at[p])
+                sent(part.at[pl.ds(0, xc - 1), pl.ds(0, first * piece)], rpsend)
+
 
         @pl.when(p != z)
         def _():
@@ -976,6 +1042,7 @@
             pltpu.VMEM((nz * (xc - 1), rows, width), bf),
             pltpu.VMEM((nz, rows, width), bf),
             pltpu.VMEM((nz, rows, width), bf),
+            pltpu.VMEM((xc - 1, rows, width), bf),
             pltpu.VMEM((rows, width), f4),
             pltpu.VMEM((n, 1, rows), f4),
             pltpu.VMEM((2, st * nt, dt), bf),
@@ -987,7 +1054,7 @@
             dma((2,)),
             dma((2, n)),
             dma((2,)),
-            dma((2, n)),
+            dma((2,)),
             dma((n,)),
             dma((n,)),
             dma((2, max(nz, nt))),
@@ -1005,6 +1072,8 @@
             dma((nz,)),
             dma((nz, PIECES)),
             dma((nz, PIECES)),
+            dma,
+            dma((xc - 1, PIECES)),
         ],
         compiler_params=pltpu.CompilerParams(
             collective_id=0, has_side_effects=True, vmem_limit_bytes=60 << 20

time: 136 us -> 135 us (level); the launches traced: 136 us -> 133 us
  Pallas kernels: 136 us -> 133 us
    pallas_call x1, Pallas kernels: 132 us -> 129 us  [kernel_plan(): pl.pallas_call(functools.partial(handover_kernel, nz, nt), out_shape=tupl...]
where the time goes in v4:
time: 135 us; the launch traced here: 133 us
  Pallas kernels  133 us (99%)
    pallas_call x1, Pallas kernels, kernel_plan(): pl.pallas_call(functools.partial(handover_kernel, nz, nt), out_shape=tupl...  129 us
    pallas_call x1, Pallas kernels, deliver(): pl.pallas_call(deliver_kernel, out_shape=tuple((jax.ShapeDtypeStruct(a.sh...  3.54 us

profile of v4, /device:TPU:0, one launch (start us, length us, event | category | flops | bytes accessed | tf_op | source)
XLA Modules:
  0.0 133.2 jit_solution(13796372362402466878)
XLA Ops:
  0.6 129.0 %shard_map.153 = (bf16[128,2048]{1,0:T(8,128)(2,1)}, bf16[2048,256]{1,0:T(8,128)(2,1)}, bf16[2048,256]{1,0:T(8,128)(2,1)}, bf16[256,2048]{1,0:T(8,128)(2,1)}, bf...) custom-call(bf16[128,2048]{1,0:T(8,128)(2,1)} %tokens.1, s32[8,128]{1,0:T(8,128)} %bitcast.14, ...), custom_call_target="tpu_custom_call" | custom-call | tf_op jit(solution)/shard_map/pallas_call | solution.py:1017
  129.7 3.5 %shard_map.154 = (bf16[128,2048]{1,0:T(8,128)(2,1)}, bf16[2048,256]{1,0:T(8,128)(2,1)}, bf16[2048,256]{1,0:T(8,128)(2,1)}, bf16[256,2048]{1,0:T(8,128)(2,1)}, bf...) custom-call(bf16[128,2048]{1,0:T(8,128)(2,1)} %get-tuple-element.21.refs_0_, ...), custom_call_target="tpu_custom_call" | custom-call | tf_op jit(solution)/shard_map/pallas_call | solution.py:972
